TPU v7x, 32 devices: a whole 2x2x4 slice. The times are simulated.
32 devices in a mesh: grp: 2 (over x), sp: 4 (over z), tp: 4 (over y, core).
Axes of the slice: x: 2, y: 2, z: 4, core: 2. Of those that a mesh axis runs over, the one named last changes fastest.
Arguments:
- tokens: bfloat16 [1792, 4096], P(('grp', 'sp'), 'tp'), parts along dimension 0, may hold values from -130 to 130
- rms_gain: float32 [2, 4096], replicated, may hold values from 0.1 to 1.9
- w_value: bfloat16 [2, 4096, 2048], P(None, 'sp', 'tp'), may hold values from -0.09375 to 0.09375
- w_gate: bfloat16 [2, 4096, 2048], P(None, 'sp', 'tp'), may hold values from -0.09375 to 0.09375
- taps: float32 [2, 31, 2048], P(None, None, 'tp'), may hold values from -8 to 8
- ln_gain: float32 [2, 2048], P(None, 'tp'), may hold values from 0.1 to 1.9
- ln_bias: float32 [2, 2048], P(None, 'tp'), may hold values from -3 to 3
- w_out: bfloat16 [2, 2048, 4096], P(None, 'sp', 'tp'), may hold values from -0.125 to 0.125
Outputs:
- result: bfloat16 [1792, 4096], P(('grp', 'sp'), 'tp'), parts along dimension 0
There are 2 independent parts, one for each index of `grp`. A program takes and returns all parts, laid end to end along the dimension named above; an argument that names none is the same for every part. Nothing has to cross between parts.
All inputs are finite; a program needn't handle non-finite values.
Results may differ from a plain program's by a relative error of at most 0.009.
Values may be sent and summed in bfloat16 or wider, within the bound.
A program may use at most 64 MiB of HBM per device.

v0:
```python
import functools

import jax
import jax.numpy as jnp
from jax import lax
from jax.experimental import pallas as pl
from jax.experimental.pallas import tpu as pltpu
from jax.sharding import PartitionSpec as P

LANES = 128
BF16, F32 = jnp.bfloat16, jnp.float32


def passed_along(block, axis, distance):
    devices = range(lax.axis_size(axis))
    route = [(i - distance, i) for i in devices if i - distance in devices]
    return lax.ppermute(block, axis, route)


def norm_rows(wide, gain):
    return (wide * lax.rsqrt(jnp.mean(wide * wide, axis=1, keepdims=True) + 1e-06) * gain).astype(
        jnp.bfloat16
    )


def to_depth(rows):
    return lax.all_to_all(rows, "sp", split_axis=1, concat_axis=0, tiled=True)


def summed(partial):
    sp = lax.axis_size("sp")
    rows = partial.shape[0] // sp
    parts = partial.astype(jnp.bfloat16).reshape(sp, rows, partial.shape[1])
    parts = lax.all_to_all(parts, "sp", split_axis=0, concat_axis=0, tiled=True)
    return jnp.sum(parts.astype(jnp.float32), axis=0)


def send(src, dst, send_sem, recv_sem, **where):
    return pltpu.make_async_remote_copy(
        src_ref=src,
        dst_ref=dst,
        send_sem=send_sem,
        recv_sem=recv_sem,
        device_id=where,
        device_id_type=pl.DeviceIdType.MESH,
    )


def gated_conv(
    layer, sp, tp,
    h_ref, gain_ref, wv_hbm, wg_hbm, taps_ref, lng_ref, lnb_ref, wo_hbm, out_ref,
    wv, wg, wo, pieces, spread, xs, going, coming, own, sq, stat, halo_out, halo_in, ext, conv, acts,
    w_sem, a_send, a_recv, b_send, c_send, c_relay, x_recv, r_send, r_recv,
    q_send, q_recv, s_send, s_recv, h_send, h_recv, g_send, g_relay, g_recv,
    o_sem, z_send, z_recv, y_send, y_recv,
):
    s, c, g = lax.axis_index("sp"), lax.axis_index("tp"), lax.axis_index("grp")
    grp, share = wo.shape[1], wo.shape[2]
    padded = sq.shape[2]
    rows, depth = h_ref.shape
    chans = taps_ref.shape[2]
    part = depth // tp
    step = going.shape[-1]
    chunks = chans // step
    pairs = tp // 2
    sibling = c + 1 - 2 * (c % 2)
    reach = taps_ref.shape[1]
    pad = halo_in.shape[0]

    loads = [
        pltpu.make_async_copy(wv_hbm.at[layer], wv, w_sem.at[0]),
        pltpu.make_async_copy(wg_hbm.at[layer], wg, w_sem.at[1]),
    ]
    for n in range(grp):
        loads.append(
            pltpu.make_async_copy(
                wo_hbm.at[layer, pl.ds(n * share, share)], wo.at[s, n], o_sem.at[n]
            )
        )
    for load in loads:
        load.start()

    barrier = pltpu.get_barrier_semaphore()
    for j in range(1, tp):
        pl.semaphore_signal(
            barrier, inc=1, device_id={"tp": (c + j) % tp}, device_id_type=pl.DeviceIdType.MESH
        )
    for j in range(1, sp):
        pl.semaphore_signal(
            barrier, inc=1, device_id={"sp": (s + j) % sp}, device_id_type=pl.DeviceIdType.MESH
        )
    for j in range(1, grp):
        pl.semaphore_signal(
            barrier, inc=1, device_id={"grp": (g + j) % grp}, device_id_type=pl.DeviceIdType.MESH
        )

    def to_row(column):
        column = jnp.concatenate([column, jnp.zeros((padded - rows, LANES), F32)], axis=0)
        return jnp.sum(column.T, axis=0, keepdims=True)

    def to_column(row):
        return jnp.broadcast_to(row, (LANES, padded)).T[:rows, 0:1]

    total = jnp.zeros((rows, LANES), F32)
    for p in range(tp):
        for lane in range(0, part, LANES):
            at = p * part + lane
            wide = h_ref[:, at : at + LANES].astype(F32)
            total = total + wide * wide
            pieces[p, :, lane : lane + LANES] = (
                wide * gain_ref[layer : layer + 1, pl.ds(pl.multiple_of(c * depth + at, LANES), LANES)]
            ).astype(BF16)
    sq[c] = jnp.broadcast_to(to_row(total), sq.shape[1:])
    spread[c] = pieces[c]
    pl.semaphore_wait(barrier, tp + sp + grp - 3)

    def a_copy(to, frm):
        return send(pieces.at[to], spread.at[frm], a_send.at[to], a_recv.at[frm], tp=to)

    def q_copy(to, frm):
        return send(sq.at[frm], sq.at[frm], q_send.at[to], q_recv.at[frm], tp=to)

    for j in range(1, tp):
        a_copy((c + j) % tp, c).start()
    for j in range(1, tp):
        q_copy((c + j) % tp, c).start()

    def z_copy(left, o):
        return send(
            wo.at[o, g], wo.at[o, g], z_send.at[left, o], z_recv.at[o], sp=s + 1 - 2 * left
        )

    def y_copy(j, o, n):
        return send(
            wo.at[o, n], wo.at[o, n], y_send.at[j, o], y_recv.at[o, n], grp=(g + j) % grp
        )

    def pass_on(i):
        for left in range(2):
            o = s + (2 * left - 1) * i

            @pl.when((o >= 0) & (o < sp))
            def _():
                send(
                    wo.at[o, g], wo.at[o, g], z_send.at[left, o], z_recv.at[o], sp=(s + 1) % sp
                ).wait_recv()

                @pl.when((1 - left) * (sp - 1 - s) + left * s > 0)
                def _():
                    z_copy(left, o).start()

                for j in range(1, grp):
                    y_copy(j, o, g).start()

    for load in loads[2:]:
        load.wait()

    @pl.when(s < sp - 1)
    def _():
        z_copy(0, s).start()

    @pl.when(s > 0)
    def _():
        z_copy(1, s).start()

    def b_copy(to, frm):
        return send(spread.at[to], xs.at[c, frm], b_send.at[to], x_recv.at[c, frm], sp=to)

    def place(j):
        left = (j + 2 * s // sp) % 2
        k = j // 2
        d = (1 - left) * (sp - 1 - k) + left * k
        return left, d, (1 - 2 * left) * (d - s) > 0

    def each(body, between=lambda j: None):
        def one(j, carry):
            left, d, valid = place(j)
            between(j)

            @pl.when(valid)
            def _():
                body(j, left, d)

            return carry

        lax.fori_loop(0, 2 * (sp - 1), one, 0)

    def held(e):
        @pl.when(e != c)
        def _():
            a_copy(c, e).wait_recv()

    def scatter(j, left, d):
        held(d)
        b_copy(d, s).start()

    each(scatter)
    held(s)
    xs[c, s] = spread[s]

    def c_copy(to, d, sem):
        return send(xs.at[c, d], xs.at[c, d], sem, x_recv.at[c, d], tp=to)

    def relay(p, d):
        return send(xs.at[p, d], xs.at[p, d], c_relay.at[p, d], x_recv.at[p, d], tp=sibling)

    def arrived(p, d):
        send(xs.at[p, d], xs.at[p, d], c_relay.at[p, d], x_recv.at[p, d], tp=sibling).wait_recv()

    def gather(d):
        @pl.when(d != s)
        def _():
            arrived(c, d)

        for j in range(1, pairs):
            c_copy((c + 2 * j) % tp, d, c_send.at[j, d]).start()
        c_copy(sibling, d, c_send.at[0, d]).start()

    each(lambda j, left, d: gather(d))
    gather(s)
    pass_on(1)
    for load in loads[:2]:
        load.wait()

    def ready(d):
        for j in range(1, pairs):
            p = (c + 2 * j) % tp
            arrived(p, d)
            relay(p, d).start()
        for j in range(pairs):
            arrived((sibling + 2 * j) % tp, d)

    def product(d, weight, at):
        acc = jnp.zeros((rows, step), F32)
        for p in range(tp):
            acc = acc + jnp.dot(
                xs[p, d],
                weight[p * part : (p + 1) * part, pl.ds(at, step)],
                preferred_element_type=F32,
            )
        return acc

    def r_copy(left, d, slot):
        return send(
            going.at[left, d, slot],
            coming.at[left, d, slot],
            r_send.at[left, d, slot],
            r_recv.at[left, d, slot],
            sp=s + 1 - 2 * left,
        )

    def r_arrived(left, d, slot):
        send(
            going.at[left, d, slot],
            coming.at[left, d, slot],
            r_send.at[left, d, slot],
            r_recv.at[left, d, slot],
            sp=(s + 1) % sp,
        ).wait_recv()

    def upstream(left):
        return (1 - left) * s + left * (sp - 1 - s) > 0

    def partial(j, left, d):
        ready(d)
        for half, weight in enumerate((wv, wg)):

            def one(i, carry):
                slot = half * chunks + i
                own[half] = product(d, weight, pl.multiple_of(i * step, step))

                @pl.when(upstream(left))
                def _():
                    r_arrived(left, d, slot)
                    own[half] += coming[left, d, slot].astype(F32)

                going[left, d, slot] = own[half].astype(BF16)
                r_copy(left, d, slot).start()
                return carry

            lax.fori_loop(0, chunks, one, 0)

    def between(j):
        for i in range(2, sp - 1):

            @pl.when(j == 2 * i)
            def _():
                pass_on(i)

    each(partial, between)
    pass_on(sp - 1)
    ready(s)
    for j in range(1, tp):
        q_copy(c, (c + j) % tp).wait_recv()
    squares = sq[0]
    for p in range(1, tp):
        squares = squares + sq[p]
    scale = to_column(lax.rsqrt(squares[0:1] / (depth * tp) + 1e-06))

    def finish(i, carry):
        at = pl.multiple_of(i * step, step)
        for half, weight in enumerate((wv, wg)):
            slot = half * chunks + i
            own[half] = product(s, weight, at)
            for left in range(2):

                @pl.when(upstream(left))
                def _():
                    r_arrived(left, s, slot)
                    own[half] += coming[left, s, slot].astype(F32)

        glu = (own[0] * scale * jax.nn.sigmoid(own[1] * scale)).astype(BF16)
        ext[pad:, pl.ds(at, step)] = glu.astype(F32)
        halo_out[:, pl.ds(at, step)] = glu[rows - pad :]
        return carry

    lax.fori_loop(0, chunks, finish, 0)

    def h_copy(to):
        return send(halo_out, halo_in, h_send, h_recv, sp=to)

    @pl.when(s < sp - 1)
    def _():
        h_copy(s + 1).start()

    @pl.when(s > 0)
    def _():
        h_copy((s + 1) % sp).wait_recv()
        ext[:pad] = halo_in[...].astype(F32)

    @pl.when(s == 0)
    def _():
        ext[:pad] = jnp.zeros((pad, chans), F32)

    first = pad - (reach - 1)

    def convolve(i, carry):
        lanes = pl.ds(pl.multiple_of(i * LANES, LANES), LANES)
        acc = jnp.zeros((rows, LANES), F32)
        for k in range(reach):
            acc = acc + taps_ref[layer, k : k + 1, lanes] * ext[first + k : first + k + rows, lanes]
        conv[:, lanes] = acc
        return carry

    lax.fori_loop(0, chans // LANES, convolve, 0)
    total = jnp.zeros((rows, LANES), F32)
    total_sq = jnp.zeros((rows, LANES), F32)
    for at in range(0, chans, LANES):
        tile = conv[:, at : at + LANES]
        total = total + tile
        total_sq = total_sq + tile * tile
    half = sq.shape[1] // 2
    stat[c] = jnp.concatenate(
        [jnp.broadcast_to(to_row(t), (half, padded)) for t in (total, total_sq)], axis=0
    )

    def s_copy(to, frm):
        return send(stat.at[frm], stat.at[frm], s_send.at[to], s_recv.at[frm], tp=to)

    for j in range(1, tp):
        s_copy((c + j) % tp, c).start()
    for j in range(1, tp):
        s_copy(c, (c + j) % tp).wait_recv()
    stats = stat[0]
    for p in range(1, tp):
        stats = stats + stat[p]
    mean = stats[0:1] / (chans * tp)
    var = stats[half : half + 1] / (chans * tp) - mean * mean
    inv = to_column(lax.rsqrt(var + 1e-05))
    mean = to_column(mean)
    for at in range(0, chans, LANES):
        lanes = slice(at, at + LANES)
        shaped = (conv[:, lanes] - mean) * inv * lng_ref[layer : layer + 1, lanes] + lnb_ref[layer : layer + 1, lanes]
        acts[c, :, lanes] = (shaped / (1.0 + jnp.exp(-shaped))).astype(BF16)

    def g_copy(to, p, sem):
        return send(acts.at[p], acts.at[p], sem, g_recv.at[p], tp=to)

    for j in range(1, pairs):
        g_copy((c + 2 * j) % tp, c, g_send.at[j]).start()
    g_copy(sibling, c, g_send.at[0]).start()
    for j in range(1, pairs):
        p = (c + 2 * j) % tp
        g_copy(sibling, p, g_relay.at[p]).wait_recv()
        g_copy(sibling, p, g_relay.at[p]).start()
    for j in range(pairs):
        p = (sibling + 2 * j) % tp
        g_copy(sibling, p, g_relay.at[p]).wait_recv()
    for i in range(1, sp):
        for left in range(2):
            o = s + (2 * left - 1) * i

            @pl.when((o >= 0) & (o < sp))
            def _():
                for j in range(1, grp):
                    y_copy(j, o, (g + j) % grp).wait_recv()

    def project(i, carry):
        lanes = pl.ds(pl.multiple_of(i * step, step), step)
        acc = jnp.zeros((rows, step), F32)
        for p in range(tp):
            for n in range(grp):
                acc = acc + jnp.dot(
                    acts[p, :, n * share : (n + 1) * share],
                    wo[p, n, :, lanes],
                    preferred_element_type=F32,
                )
        out_ref[:, lanes] = (h_ref[:, lanes].astype(F32) + acc).astype(BF16)
        return carry

    lax.fori_loop(0, depth // step, project, 0)

    for j in range(1, tp):
        a_copy((c + j) % tp, c).wait_send()
        q_copy((c + j) % tp, c).wait_send()
        s_copy((c + j) % tp, c).wait_send()
    for j in range(1, sp):
        b_copy((s + j) % sp, s).wait_send()

    def sent(d, carry):
        c_copy(sibling, d, c_send.at[0, d]).wait_send()
        for j in range(1, pairs):
            p = (c + 2 * j) % tp
            c_copy(p, d, c_send.at[j, d]).wait_send()
            relay(p, d).wait_send()
        return carry

    lax.fori_loop(0, sp, sent, 0)

    def partial_sent(j, left, d):
        def one(slot, carry):
            r_copy(left, d, slot).wait_send()
            return carry

        lax.fori_loop(0, 2 * chunks, one, 0)

    each(partial_sent)

    @pl.when(s < sp - 1)
    def _():
        h_copy(s + 1).wait_send()
        z_copy(0, s).wait_send()

    @pl.when(s > 0)
    def _():
        z_copy(1, s).wait_send()

    for i in range(1, sp):
        for left in range(2):
            o = s + (2 * left - 1) * i

            @pl.when((o >= 0) & (o < sp))
            def _():
                @pl.when((1 - left) * (sp - 1 - s) + left * s > 0)
                def _():
                    z_copy(left, o).wait_send()

                for j in range(1, grp):
                    y_copy(j, o, g).wait_send()

    g_copy(sibling, c, g_send.at[0]).wait_send()
    for j in range(1, pairs):
        p = (c + 2 * j) % tp
        g_copy(p, c, g_send.at[j]).wait_send()
        g_copy(sibling, p, g_relay.at[p]).wait_send()


def fused_layer(layer, h, gain, w_value, w_gate, taps, ln_gain, ln_bias, w_out):
    sp, tp, grp = (lax.axis_size(a) for a in ("sp", "tp", "grp"))
    rows, depth = h.shape
    padded = -(-rows // LANES) * LANES
    chans, reach = w_value.shape[2], taps.shape[1]
    part, step = depth // tp, min(2 * LANES, chans)
    slots = 2 * (chans // step)
    pad = -(-(reach - 1) // 16) * 16
    vmem, dma = pltpu.VMEM, pltpu.SemaphoreType.DMA
    here = pl.BlockSpec(memory_space=pltpu.VMEM)
    there = pl.BlockSpec(memory_space=pl.ANY)
    return pl.pallas_call(
        functools.partial(gated_conv, layer, sp, tp),
        out_shape=jax.ShapeDtypeStruct((rows, depth), BF16),
        in_specs=[here, here, there, there, here, here, here, there],
        out_specs=here,
        scratch_shapes=[
            vmem((depth, chans), BF16),
            vmem((depth, chans), BF16),
            vmem((sp, grp, w_out.shape[1] // grp, depth), BF16),
            vmem((tp, rows, part), BF16),
            vmem((tp, rows, part), BF16),
            vmem((tp, sp, rows, part), BF16),
            vmem((2, sp, slots, rows, step), BF16),
            vmem((2, sp, slots, rows, step), BF16),
            vmem((2, rows, step), F32),
            vmem((tp, 8, padded), F32),
            vmem((tp, 8, padded), F32),
            vmem((pad, chans), BF16),
            vmem((pad, chans), BF16),
            vmem((pad + rows, chans), F32),
            vmem((rows, chans), F32),
            vmem((tp, rows, chans), BF16),
            dma((2,)), dma((tp,)), dma((tp,)), dma((sp,)), dma((tp, sp)), dma((tp, sp)),
            dma((tp, sp)), dma((2, sp, slots)), dma((2, sp, slots)),
            dma((tp,)), dma((tp,)), dma((tp,)), dma((tp,)), dma, dma,
            dma((tp,)), dma((tp,)), dma((tp,)),
            dma((grp,)), dma((2, sp)), dma((sp,)), dma((grp, sp)), dma((sp, grp)),
        ],
        compiler_params=pltpu.CompilerParams(
            collective_id=layer, has_side_effects=True, vmem_limit_bytes=48 * 2**20
        ),
    )(h, gain, w_value, w_gate, taps, ln_gain, ln_bias, w_out)


def fits(tokens, w_value, taps):
    sp, tp, grp = (lax.axis_size(a) for a in ("sp", "tp", "grp"))
    rows, depth = tokens.shape
    chans = w_value.shape[2]
    return (
        sp == tp
        and tp % 2 == 0
        and depth % (tp * LANES) == 0
        and chans % (LANES * grp) == 0
        and chans % min(2 * LANES, chans) == 0
        and rows % 16 == 0
        and rows >= -(-(taps.shape[1] - 1) // 16) * 16
    )


def fused(tokens, rms_gain, w_value, w_gate, taps, ln_gain, ln_bias, w_out):
    current = tokens
    for layer in range(w_value.shape[0]):
        current = fused_layer(
            layer, current, rms_gain, w_value, w_gate, taps, ln_gain, ln_bias, w_out
        )
    return current


def shards(tokens, rms_gain, w_value, w_gate, taps, ln_gain, ln_bias, w_out):
    if fits(tokens, w_value, taps):
        return fused(tokens, rms_gain, w_value, w_gate, taps, ln_gain, ln_bias, w_out)
    layers = w_value.shape[0]
    tok_rows = tokens.shape[0]
    chans = w_value.shape[2]
    all_chans = chans * lax.axis_size("tp")
    reach = taps.shape[1]
    current = tokens
    for layer in range(layers):
        whole_rows = lax.all_gather(current, "tp", axis=1, tiled=True)
        normed = to_depth(norm_rows(whole_rows.astype(jnp.float32), rms_gain[layer]))
        both = jnp.concatenate([w_value[layer], w_gate[layer]], axis=1)
        both = summed(jnp.dot(normed, both, preferred_element_type=jnp.float32))
        glu = (both[:, :chans] * jax.nn.sigmoid(both[:, chans:])).astype(jnp.bfloat16)
        earlier = passed_along(glu[tok_rows - (reach - 1) :], "sp", 1)
        extended = jnp.concatenate([earlier, glu], axis=0).astype(jnp.float32)
        conv = jnp.zeros((tok_rows, chans), jnp.float32)
        for k in range(reach):
            conv = conv + taps[layer, k][None, :] * extended[k : k + tok_rows]
        total, total_sq = lax.psum((jnp.sum(conv, axis=1), jnp.sum(conv * conv, axis=1)), "tp")
        mean = total / all_chans
        var = total_sq / all_chans - mean * mean
        shaped = (conv - mean[:, None]) * lax.rsqrt(var + 1e-05)[:, None] * ln_gain[layer][
            None, :
        ] + ln_bias[layer][None, :]
        act = jax.nn.silu(shaped).astype(jnp.bfloat16)
        act_all = to_depth(lax.all_gather(act, "tp", axis=1, tiled=True))
        branch = summed(jnp.dot(act_all, w_out[layer], preferred_element_type=jnp.float32))
        current = (current.astype(jnp.float32) + branch).astype(jnp.bfloat16)
    return current


def solution(mesh):
    return jax.shard_map(
        shards,
        mesh=mesh,
        in_specs=(
            P(("grp", "sp"), "tp"),
            P(),
            P(None, "sp", "tp"),
            P(None, "sp", "tp"),
            P(None, None, "tp"),
            P(None, "tp"),
            P(None, "tp"),
            P(None, "sp", "tp"),
        ),
        out_specs=P(("grp", "sp"), "tp"),
        check_vma=False,
    )
```

profile of v0, /device:TPU:15, one launch (start us, length us, event | category | flops | bytes accessed | tf_op | source)
XLA Modules:
  0.0 180.4 jit_solution(863786590878342880)
XLA Ops:
  0.0 0.9 copy.9.taps_ref
  0.9 0.0 copy-start
  0.9 1.6 copy-done
  2.5 0.0 copy-start.2
  2.5 1.6 copy-done.2
  4.1 0.0 copy-start.4
  4.1 1.0 copy-done.4
  5.1 0.0 copy-start.5
  5.1 0.8 copy-done.5
  5.9 0.0 copy-start.6
  5.9 0.7 copy-done.6
  6.6 0.0 copy-start.7
  6.6 0.7 copy-done.7
  7.3 0.0 copy-start.1
  7.3 0.0 copy-start.3
  7.3 85.9 %shard_map.82.h_ref = bf16[224,1024]{1,0:T(8,128)(2,1)S(1)} custom-call(bf16[224,1024]{1,0:T(8,128)(2,1)S(1)} %copy-done.4, f32[2,4096]{1,0:T(2,128)S(1)} %copy-done.5, bf16[2,1024,512]{2,1,0:T(8,128)(2,1)S(1)} %copy-done, bf16[2,1024,512]{2,1,0:T(8,128)(2,1)S(1)} %copy-done.2, f32[2,31,512]{2,1,0:T(8,128)S(1)} %copy.9.taps_ref, f32[2,512]{1,0:T(2,128)S(1)} %copy-done.6, ...), custom_call_target="tpu_custom_call" | custom-call | tf_op jit(solution)/shard_map/pallas_call | solution.py:479
  93.2 0.0 copy-done.1
  93.2 0.0 copy-done.3
  93.2 86.4 %shard_map.83 = bf16[224,1024]{1,0:T(8,128)(2,1)S(1)} custom-call(bf16[224,1024]{1,0:T(8,128)(2,1)S(1)} %shard_map.82.h_ref, f32[2,4096]{1,0:T(2,128)S(1)} %copy-done.5, bf16[2,1024,512]{2,1,0:T(8,128)(2,1)S(1)} %copy-done.1, bf16[2,1024,512]{2,1,0:T(8,128)(2,1)S(1)} %copy-done.3, f32[2,31,512]{2,1,0:T(8,128)S(1)} %copy.9.taps_ref, f32[2,512]{1,0:T(2,128)S(1)} %copy-done.6, ...), custom_call_target="tpu_custom_call" | custom-call | tf_op jit(solution)/shard_map/pallas_call | solution.py:479
  179.6 0.8 copy.12
Async XLA Ops:
  0.9 1.6 copy-start
  2.5 1.6 copy-start.2
  4.1 1.0 copy-start.4
  5.1 0.8 copy-start.5
  5.9 0.7 copy-start.6
  6.6 0.7 copy-start.7
  7.3 85.9 %copy-start.1 = (bf16[2,1024,512]{2,1,0:T(8,128)(2,1)S(1)}, bf16[2,1024,512]{2,1,0:T(8,128)(2,1)}, u32[]{:S(2)}) copy-start(bf16[2,1024,512]{2,1,0:T(8,128)(2,1)} %wv_hbm.3) | copy-start | bytes 6291460
  7.3 85.9 %copy-start.3 = (bf16[2,1024,512]{2,1,0:T(8,128)(2,1)S(1)}, bf16[2,1024,512]{2,1,0:T(8,128)(2,1)}, u32[]{:S(2)}) copy-start(bf16[2,1024,512]{2,1,0:T(8,128)(2,1)} %wg_hbm.3) | copy-start | bytes 6291460
where the time goes:
time: 181 us; the launch traced here: 180 us
  Pallas kernels  172 us (95%)
  local copies, waits for them, and re-layouts  8.03 us (4%)
    pallas_call x2, Pallas kernels, fused_layer(): pl.pallas_call(functools.partial(gated_conv, layer, sp, tp), out_shape=ja...  172 us
    unnamed x18, local copies, waits for them, and re-layouts  8.03 us

commit v1 on v0

v1 whole, which is shorter than its diff:
```python
import functools

import jax
import jax.numpy as jnp
from jax import lax
from jax.experimental import pallas as pl
from jax.experimental.pallas import tpu as pltpu
from jax.sharding import PartitionSpec as P

LANES = 128
BF16, F32 = jnp.bfloat16, jnp.float32
CUTS = 4


def passed_along(block, axis, distance):
    devices = range(lax.axis_size(axis))
    route = [(i - distance, i) for i in devices if i - distance in devices]
    return lax.ppermute(block, axis, route)


def norm_rows(wide, gain):
    return (wide * lax.rsqrt(jnp.mean(wide * wide, axis=1, keepdims=True) + 1e-06) * gain).astype(
        jnp.bfloat16
    )


def to_depth(rows):
    return lax.all_to_all(rows, "sp", split_axis=1, concat_axis=0, tiled=True)


def summed(partial):
    sp = lax.axis_size("sp")
    rows = partial.shape[0] // sp
    parts = partial.astype(jnp.bfloat16).reshape(sp, rows, partial.shape[1])
    parts = lax.all_to_all(parts, "sp", split_axis=0, concat_axis=0, tiled=True)
    return jnp.sum(parts.astype(jnp.float32), axis=0)


def send(src, dst, send_sem, recv_sem, **where):
    return pltpu.make_async_remote_copy(
        src_ref=src,
        dst_ref=dst,
        send_sem=send_sem,
        recv_sem=recv_sem,
        device_id=where,
        device_id_type=pl.DeviceIdType.MESH,
    )


def gated_conv(
    layers, sp, tp,
    h_hbm, gain_hbm, wv_hbm, wg_hbm, taps_hbm, lng_hbm, lnb_hbm, wo_hbm, out_ref,
    h_ref, gain_ref, taps_ref, lng_ref, lnb_ref, mid,
    wv, wg, wo, pieces, spread, xs, going, coming, own, sq, sq_sum, stat,
    halo_out, halo_in, ext, conv, acts,
    i_sem, w_sem, a_send, a_recv, b_send, c_send, c_relay, x_recv, r_send, r_recv,
    q_send, q_recv, s_send, s_recv, h_send, h_recv, g_send, g_relay, g_recv,
    o_sem, z_send, z_recv, y_send, y_recv,
):
    s, c, g = lax.axis_index("sp"), lax.axis_index("tp"), lax.axis_index("grp")
    grp, share = wo.shape[2], wo.shape[3]
    padded = sq.shape[3]
    rows, depth = h_ref.shape
    chans = taps_ref.shape[2]
    part = depth // tp
    step = going.shape[-1]
    chunks = chans // step
    pairs = tp // 2
    sibling = c + 1 - 2 * (c % 2)
    reach = taps_ref.shape[0]
    pad = halo_in.shape[1]
    cuts = z_recv.shape[2]
    early = cuts // 2
    cut = share // cuts

    first_loads = [
        pltpu.make_async_copy(h_hbm, h_ref, i_sem.at[0]),
        pltpu.make_async_copy(
            gain_hbm.at[:, pl.ds(pl.multiple_of(c * depth, LANES), depth)], gain_ref, i_sem.at[1]
        ),
    ]
    small_loads = [
        pltpu.make_async_copy(taps_hbm, taps_ref, i_sem.at[2]),
        pltpu.make_async_copy(lng_hbm, lng_ref, i_sem.at[3]),
        pltpu.make_async_copy(lnb_hbm, lnb_ref, i_sem.at[4]),
    ]
    in_loads = [
        (
            pltpu.make_async_copy(wv_hbm.at[l], wv.at[l], w_sem.at[l, 0]),
            pltpu.make_async_copy(wg_hbm.at[l], wg.at[l], w_sem.at[l, 1]),
        )
        for l in range(layers)
    ]
    out_loads = [
        [
            pltpu.make_async_copy(
                wo_hbm.at[l, pl.ds(n * share, share)], wo.at[l, s, n], o_sem.at[l, n]
            )
            for n in range(grp)
        ]
        for l in range(layers)
    ]
    for load in first_loads:
        load.start()
    for l in range(layers):
        for load in out_loads[l]:
            load.start()
        for load in in_loads[l]:
            load.start()
    for load in small_loads:
        load.start()

    barrier = pltpu.get_barrier_semaphore()
    for j in range(1, tp):
        pl.semaphore_signal(
            barrier, inc=1, device_id={"tp": (c + j) % tp}, device_id_type=pl.DeviceIdType.MESH
        )
    for j in range(1, sp):
        pl.semaphore_signal(
            barrier, inc=1, device_id={"sp": (s + j) % sp}, device_id_type=pl.DeviceIdType.MESH
        )
    for j in range(1, grp):
        pl.semaphore_signal(
            barrier, inc=1, device_id={"grp": (g + j) % grp}, device_id_type=pl.DeviceIdType.MESH
        )

    def to_row(column):
        column = jnp.concatenate([column, jnp.zeros((padded - rows, LANES), F32)], axis=0)
        return jnp.sum(column.T, axis=0, keepdims=True)

    def to_column(row):
        return jnp.broadcast_to(row, (LANES, padded)).T[:rows, 0:1]

    def turn(i):
        return ((c // 2 + 1 + i // 2) % pairs) * 2 + (c + 1 + i) % 2

    def a_copy(l, to, frm):
        return send(
            pieces.at[l, to], spread.at[l, frm], a_send.at[l, to], a_recv.at[l, frm], tp=to
        )

    def q_copy(l, to, frm):
        return send(sq.at[l, frm], sq.at[l, frm], q_send.at[l, to], q_recv.at[l, frm], tp=to)

    def prepare(l, p, block):
        wide = block.astype(F32)
        total = sq_sum[...]
        for lane in range(0, part, LANES):
            tile = wide[:, lane : lane + LANES]
            total = total + tile * tile
        sq_sum[...] = total
        gain = gain_ref[l : l + 1, pl.ds(pl.multiple_of(p * part, LANES), part)]
        pieces[l, p] = (wide * gain).astype(BF16)

    def hand_out(l, p):
        @pl.when(p != c)
        def _():
            a_copy(l, p, c).start()

        @pl.when(p == c)
        def _():
            spread[l, c] = pieces[l, c]

    def hand_out_squares(l):
        sq[l, c] = jnp.broadcast_to(to_row(sq_sum[...]), sq.shape[2:])
        for j in range(1, tp):
            q_copy(l, (c + j) % tp, c).start()

    def beyond(left):
        return (1 - left) * (sp - 1 - s) + left * s

    def z_copy(l, left, o, k):
        rows_k = pl.ds(k * cut, cut)
        return send(
            wo.at[l, o, g, rows_k],
            wo.at[l, o, g, rows_k],
            z_send.at[l, left, o, k],
            z_recv.at[l, o, k],
            sp=s + 1 - 2 * left,
        )

    def y_copy(l, j, o, n, k):
        rows_k = pl.ds(k * cut, cut)
        return send(
            wo.at[l, o, n, rows_k],
            wo.at[l, o, n, rows_k],
            y_send.at[l, j, o, k],
            y_recv.at[l, o, n, k],
            grp=(g + j) % grp,
        )

    def z_own(l, left, k):
        @pl.when(beyond(left) > 0)
        def _():
            z_copy(l, left, s, k).start()

    def z_pass(l, left, i, k):
        o = s + (2 * left - 1) * i

        @pl.when((o >= 0) & (o < sp))
        def _():
            rows_k = pl.ds(k * cut, cut)
            send(
                wo.at[l, o, g, rows_k],
                wo.at[l, o, g, rows_k],
                z_send.at[l, left, o, k],
                z_recv.at[l, o, k],
                sp=(s + 1) % sp,
            ).wait_recv()

            @pl.when(beyond(left) > 0)
            def _():
                z_copy(l, left, o, k).start()

            for j in range(1, grp):
                y_copy(l, j, o, g, k).start()

    def z_rest(l, lean):
        for left in range(2):

            @pl.when((beyond(left) <= 1) == lean)
            def _():
                for k in range(early if l == 0 else cuts, cuts):
                    z_own(l, left, k)
                for k in range(early):
                    z_pass(l, left, 1, k)

    def place(j):
        left = (j + 2 * s // sp) % 2
        k = j // 2
        d = (1 - left) * (sp - 1 - k) + left * k
        return left, d, (1 - 2 * left) * (d - s) > 0

    def each(body):
        def one(j, carry):
            left, d, valid = place(j)

            @pl.when(valid)
            def _():
                body(j, left, d)

            return carry

        lax.fori_loop(0, 2 * (sp - 1), one, 0)

    def upstream(left):
        return (1 - left) * s + left * (sp - 1 - s) > 0

    def b_copy(l, to, frm):
        return send(
            spread.at[l, to], xs.at[l, c, frm], b_send.at[l, to], x_recv.at[l, c, frm], sp=to
        )

    def c_copy(l, to, d, sem):
        return send(xs.at[l, c, d], xs.at[l, c, d], sem, x_recv.at[l, c, d], tp=to)

    def relay(l, p, d):
        return send(
            xs.at[l, p, d], xs.at[l, p, d], c_relay.at[l, p, d], x_recv.at[l, p, d], tp=sibling
        )

    def r_copy(l, left, d, slot):
        return send(
            going.at[l, left, d, slot],
            coming.at[l, left, d, slot],
            r_send.at[l, left, d, slot],
            r_recv.at[l, left, d, slot],
            sp=s + 1 - 2 * left,
        )

    def h_copy(l, to):
        return send(halo_out.at[l], halo_in.at[l], h_send.at[l], h_recv.at[l], sp=to)

    def s_copy(l, to, frm):
        return send(stat.at[l, frm], stat.at[l, frm], s_send.at[l, to], s_recv.at[l, frm], tp=to)

    def g_copy(l, to, p, sem):
        return send(acts.at[l, p], acts.at[l, p], sem, g_recv.at[l, p], tp=to)

    def layer_of(l):
        def held(e):
            @pl.when(e != c)
            def _():
                a_copy(l, c, e).wait_recv()

        def scatter(j, left, d):
            held(d)
            b_copy(l, d, s).start()

        each(scatter)
        held(s)
        xs[l, c, s] = spread[l, s]

        def gather(d):
            @pl.when(d != s)
            def _():
                relay(l, c, d).wait_recv()

            for j in range(1, pairs):
                c_copy(l, (c + 2 * j) % tp, d, c_send.at[l, j, d]).start()
            c_copy(l, sibling, d, c_send.at[l, 0, d]).start()

        gather(s)
        each(lambda j, left, d: gather(d))
        z_rest(l, True)
        for load in in_loads[l]:
            load.wait()

        def ready(d):
            for j in range(1, pairs):
                p = (c + 2 * j) % tp
                relay(l, p, d).wait_recv()
                relay(l, p, d).start()
            for j in range(pairs):
                relay(l, (sibling + 2 * j) % tp, d).wait_recv()

        def product(d, weight, at):
            acc = jnp.zeros((rows, step), F32)
            for p in range(tp):
                acc = acc + jnp.dot(
                    xs[l, p, d],
                    weight[l, p * part : (p + 1) * part, pl.ds(at, step)],
                    preferred_element_type=F32,
                )
            return acc

        def r_arrived(left, d, slot):
            send(
                going.at[l, left, d, slot],
                coming.at[l, left, d, slot],
                r_send.at[l, left, d, slot],
                r_recv.at[l, left, d, slot],
                sp=(s + 1) % sp,
            ).wait_recv()

        def partial(j, left, d):
            ready(d)
            for half, weight in enumerate((wv, wg)):

                def one(i, carry):
                    slot = half * chunks + i
                    own[half] = product(d, weight, pl.multiple_of(i * step, step))

                    @pl.when(upstream(left))
                    def _():
                        r_arrived(left, d, slot)
                        own[half] += coming[l, left, d, slot].astype(F32)

                    going[l, left, d, slot] = own[half].astype(BF16)
                    r_copy(l, left, d, slot).start()
                    return carry

                lax.fori_loop(0, chunks, one, 0)

        each(partial)
        z_rest(l, False)
        ready(s)
        for j in range(1, tp):
            q_copy(l, c, (c + j) % tp).wait_recv()
        squares = sq[l, 0]
        for p in range(1, tp):
            squares = squares + sq[l, p]
        scale = to_column(lax.rsqrt(squares[0:1] / (depth * tp) + 1e-06))

        def finish(i, carry):
            at = pl.multiple_of(i * step, step)
            for half, weight in enumerate((wv, wg)):
                slot = half * chunks + i
                own[half] = product(s, weight, at)
                for left in range(2):

                    @pl.when(upstream(left))
                    def _():
                        r_arrived(left, s, slot)
                        own[half] += coming[l, left, s, slot].astype(F32)

            glu = (own[0] * scale * jax.nn.sigmoid(own[1] * scale)).astype(BF16)
            ext[pad:, pl.ds(at, step)] = glu.astype(F32)
            halo_out[l, :, pl.ds(at, step)] = glu[rows - pad :]
            return carry

        lax.fori_loop(0, chunks, finish, 0)

        @pl.when(s < sp - 1)
        def _():
            h_copy(l, s + 1).start()

        for k in range(early, cuts):
            for left in range(2):
                z_pass(l, left, 1, k)

        @pl.when(s > 0)
        def _():
            h_copy(l, (s + 1) % sp).wait_recv()
            ext[:pad] = halo_in[l].astype(F32)

        @pl.when(s == 0)
        def _():
            ext[:pad] = jnp.zeros((pad, chans), F32)

        if l == 0:
            for load in small_loads:
                load.wait()
        first = pad - (reach - 1)

        def convolve(i, carry):
            lanes = pl.ds(pl.multiple_of(i * LANES, LANES), LANES)
            acc = jnp.zeros((rows, LANES), F32)
            for k in range(reach):
                acc = acc + taps_ref[k, l : l + 1, lanes] * ext[first + k : first + k + rows, lanes]
            conv[:, lanes] = acc
            return carry

        lax.fori_loop(0, chans // LANES, convolve, 0)
        total = jnp.zeros((rows, LANES), F32)
        total_sq = jnp.zeros((rows, LANES), F32)
        for at in range(0, chans, LANES):
            tile = conv[:, at : at + LANES]
            total = total + tile
            total_sq = total_sq + tile * tile
        half = sq.shape[2] // 2
        stat[l, c] = jnp.concatenate(
            [jnp.broadcast_to(to_row(t), (half, padded)) for t in (total, total_sq)], axis=0
        )
        for j in range(1, tp):
            s_copy(l, (c + j) % tp, c).start()
        for k in range(early):
            for left in range(2):
                z_pass(l, left, 2, k)
        for j in range(1, tp):
            s_copy(l, c, (c + j) % tp).wait_recv()
        stats = stat[l, 0]
        for p in range(1, tp):
            stats = stats + stat[l, p]
        mean = stats[0:1] / (chans * tp)
        var = stats[half : half + 1] / (chans * tp) - mean * mean
        inv = to_column(lax.rsqrt(var + 1e-05))
        mean = to_column(mean)
        for at in range(0, chans, LANES):
            lanes = slice(at, at + LANES)
            shaped = (conv[:, lanes] - mean) * inv * lng_ref[l : l + 1, lanes] + lnb_ref[
                l : l + 1, lanes
            ]
            acts[l, c, :, lanes] = (shaped / (1.0 + jnp.exp(-shaped))).astype(BF16)

        for j in range(1, pairs):
            g_copy(l, (c + 2 * j) % tp, c, g_send.at[l, j]).start()
        g_copy(l, sibling, c, g_send.at[l, 0]).start()
        for j in range(1, pairs):
            p = (c + 2 * j) % tp
            g_copy(l, sibling, p, g_relay.at[l, p]).wait_recv()
            g_copy(l, sibling, p, g_relay.at[l, p]).start()
        for k in range(early, cuts):
            for left in range(2):
                z_pass(l, left, 2, k)
        for i in range(3, sp):
            for k in range(cuts):
                for left in range(2):
                    z_pass(l, left, i, k)
        if l + 1 < layers:
            for load in out_loads[l + 1]:
                load.wait()
            for k in range(cuts):
                for left in range(2):
                    z_own(l + 1, left, k)
        for j in range(pairs):
            p = (sibling + 2 * j) % tp
            g_copy(l, sibling, p, g_relay.at[l, p]).wait_recv()
        for i in range(1, sp):
            for left in range(2):
                o = s + (2 * left - 1) * i

                @pl.when((o >= 0) & (o < sp))
                def _():
                    for k in range(cuts):
                        for j in range(1, grp):
                            y_copy(l, j, o, (g + j) % grp, k).wait_recv()

        sq_sum[...] = jnp.zeros_like(sq_sum)

        def project(i, carry):
            p = turn(i)
            lanes = pl.ds(pl.multiple_of(p * part, LANES), part)
            acc = jnp.zeros((rows, part), F32)
            for e in range(tp):
                for n in range(grp):
                    acc = acc + jnp.dot(
                        acts[l, e, :, n * share : (n + 1) * share],
                        wo[l, e, n, :, lanes],
                        preferred_element_type=F32,
                    )
            before = h_ref if l == 0 else mid.at[l - 1]
            block = (before[:, lanes].astype(F32) + acc).astype(BF16)
            if l + 1 < layers:
                mid[l, :, lanes] = block
                prepare(l + 1, p, block)
                hand_out(l + 1, p)
            else:
                out_ref[:, lanes] = block
            return carry

        lax.fori_loop(0, tp, project, 0)
        if l + 1 < layers:
            hand_out_squares(l + 1)

    sq_sum[...] = jnp.zeros_like(sq_sum)
    for load in first_loads:
        load.wait()
    for p in range(tp):
        prepare(0, p, h_ref[:, p * part : (p + 1) * part])
    for load in out_loads[0]:
        load.wait()
    pl.semaphore_wait(barrier, tp + sp + grp - 3)

    def first_hand_out(i, carry):
        hand_out(0, turn(i))
        return carry

    lax.fori_loop(0, tp, first_hand_out, 0)
    for k in range(early):
        for left in range(2):
            z_own(0, left, k)
    hand_out_squares(0)
    for l in range(layers):
        layer_of(l)

    for l in range(layers):
        for j in range(1, tp):
            a_copy(l, (c + j) % tp, c).wait_send()
            q_copy(l, (c + j) % tp, c).wait_send()
            s_copy(l, (c + j) % tp, c).wait_send()
        for j in range(1, sp):
            b_copy(l, (s + j) % sp, s).wait_send()

        def sent(d, carry):
            c_copy(l, sibling, d, c_send.at[l, 0, d]).wait_send()
            for j in range(1, pairs):
                p = (c + 2 * j) % tp
                c_copy(l, p, d, c_send.at[l, j, d]).wait_send()
                relay(l, p, d).wait_send()
            return carry

        lax.fori_loop(0, sp, sent, 0)

        def partial_sent(j, left, d):
            def one(slot, carry):
                r_copy(l, left, d, slot).wait_send()
                return carry

            lax.fori_loop(0, 2 * chunks, one, 0)

        each(partial_sent)

        @pl.when(s < sp - 1)
        def _():
            h_copy(l, s + 1).wait_send()

        for i in range(sp):
            for left in range(2):
                o = s + (2 * left - 1) * i

                @pl.when((o >= 0) & (o < sp))
                def _():
                    for k in range(cuts):

                        @pl.when(beyond(left) > 0)
                        def _():
                            z_copy(l, left, o, k).wait_send()

                        if i > 0:
                            for j in range(1, grp):
                                y_copy(l, j, o, g, k).wait_send()

        g_copy(l, sibling, c, g_send.at[l, 0]).wait_send()
        for j in range(1, pairs):
            p = (c + 2 * j) % tp
            g_copy(l, p, c, g_send.at[l, j]).wait_send()
            g_copy(l, sibling, p, g_relay.at[l, p]).wait_send()


def fused(tokens, rms_gain, w_value, w_gate, taps, ln_gain, ln_bias, w_out):
    sp, tp, grp = (lax.axis_size(a) for a in ("sp", "tp", "grp"))
    rows, depth = tokens.shape
    padded = -(-rows // LANES) * LANES
    layers, chans, reach = w_value.shape[0], w_value.shape[2], taps.shape[1]
    part, step = depth // tp, min(2 * LANES, chans)
    slots = 2 * (chans // step)
    pad = -(-(reach - 1) // 16) * 16
    share = w_out.shape[1] // grp
    cuts = CUTS
    vmem, dma = pltpu.VMEM, pltpu.SemaphoreType.DMA
    there = pl.BlockSpec(memory_space=pltpu.HBM)
    return pl.pallas_call(
        functools.partial(gated_conv, layers, sp, tp),
        out_shape=jax.ShapeDtypeStruct((rows, depth), BF16),
        in_specs=[there] * 8,
        out_specs=pl.BlockSpec(memory_space=pltpu.VMEM),
        scratch_shapes=[
            vmem((rows, depth), BF16),
            vmem((layers, depth), F32),
            vmem((reach, layers, chans), F32),
            vmem((layers, chans), F32),
            vmem((layers, chans), F32),
            vmem((layers, rows, depth), BF16),
            vmem((layers, depth, chans), BF16),
            vmem((layers, depth, chans), BF16),
            vmem((layers, sp, grp, share, depth), BF16),
            vmem((layers, tp, rows, part), BF16),
            vmem((layers, tp, rows, part), BF16),
            vmem((layers, tp, sp, rows, part), BF16),
            vmem((layers, 2, sp, slots, rows, step), BF16),
            vmem((layers, 2, sp, slots, rows, step), BF16),
            vmem((2, rows, step), F32),
            vmem((layers, tp, 8, padded), F32),
            vmem((rows, LANES), F32),
            vmem((layers, tp, 8, padded), F32),
            vmem((layers, pad, chans), BF16),
            vmem((layers, pad, chans), BF16),
            vmem((pad + rows, chans), F32),
            vmem((rows, chans), F32),
            vmem((layers, tp, rows, chans), BF16),
            dma((5,)), dma((layers, 2)),
            dma((layers, tp)), dma((layers, tp)), dma((layers, sp)),
            dma((layers, tp, sp)), dma((layers, tp, sp)), dma((layers, tp, sp)),
            dma((layers, 2, sp, slots)), dma((layers, 2, sp, slots)),
            dma((layers, tp)), dma((layers, tp)), dma((layers, tp)), dma((layers, tp)),
            dma((layers,)), dma((layers,)),
            dma((layers, tp)), dma((layers, tp)), dma((layers, tp)),
            dma((layers, grp)), dma((layers, 2, sp, cuts)), dma((layers, sp, cuts)),
            dma((layers, grp, sp, cuts)), dma((layers, sp, grp, cuts)),
        ],
        compiler_params=pltpu.CompilerParams(
            collective_id=0, has_side_effects=True, vmem_limit_bytes=60 * 2**20
        ),
    )(
        tokens, rms_gain, w_value, w_gate, jnp.transpose(taps, (1, 0, 2)), ln_gain, ln_bias, w_out
    )


def fits(tokens, w_value, taps, w_out):
    sp, tp, grp = (lax.axis_size(a) for a in ("sp", "tp", "grp"))
    rows, depth = tokens.shape
    chans = w_value.shape[2]
    return (
        sp == tp
        and tp % 2 == 0
        and depth % (tp * LANES) == 0
        and chans % (LANES * grp) == 0
        and w_out.shape[1] % (16 * grp * CUTS) == 0
        and w_out.shape[1] == chans
        and chans % min(2 * LANES, chans) == 0
        and rows % 16 == 0
        and rows >= -(-(taps.shape[1] - 1) // 16) * 16
    )


def shards(tokens, rms_gain, w_value, w_gate, taps, ln_gain, ln_bias, w_out):
    if fits(tokens, w_value, taps, w_out):
        return fused(tokens, rms_gain, w_value, w_gate, taps, ln_gain, ln_bias, w_out)
    layers = w_value.shape[0]
    tok_rows = tokens.shape[0]
    chans = w_value.shape[2]
    all_chans = chans * lax.axis_size("tp")
    reach = taps.shape[1]
    current = tokens
    for layer in range(layers):
        whole_rows = lax.all_gather(current, "tp", axis=1, tiled=True)
        normed = to_depth(norm_rows(whole_rows.astype(jnp.float32), rms_gain[layer]))
        both = jnp.concatenate([w_value[layer], w_gate[layer]], axis=1)
        both = summed(jnp.dot(normed, both, preferred_element_type=jnp.float32))
        glu = (both[:, :chans] * jax.nn.sigmoid(both[:, chans:])).astype(jnp.bfloat16)
        earlier = passed_along(glu[tok_rows - (reach - 1) :], "sp", 1)
        extended = jnp.concatenate([earlier, glu], axis=0).astype(jnp.float32)
        conv = jnp.zeros((tok_rows, chans), jnp.float32)
        for k in range(reach):
            conv = conv + taps[layer, k][None, :] * extended[k : k + tok_rows]
        total, total_sq = lax.psum((jnp.sum(conv, axis=1), jnp.sum(conv * conv, axis=1)), "tp")
        mean = total / all_chans
        var = total_sq / all_chans - mean * mean
        shaped = (conv - mean[:, None]) * lax.rsqrt(var + 1e-05)[:, None] * ln_gain[layer][
            None, :
        ] + ln_bias[layer][None, :]
        act = jax.nn.silu(shaped).astype(jnp.bfloat16)
        act_all = to_depth(lax.all_gather(act, "tp", axis=1, tiled=True))
        branch = summed(jnp.dot(act_all, w_out[layer], preferred_element_type=jnp.float32))
        current = (current.astype(jnp.float32) + branch).astype(jnp.bfloat16)
    return current


def solution(mesh):
    return jax.shard_map(
        shards,
        mesh=mesh,
        in_specs=(
            P(("grp", "sp"), "tp"),
            P(),
            P(None, "sp", "tp"),
            P(None, "sp", "tp"),
            P(None, None, "tp"),
            P(None, "tp"),
            P(None, "tp"),
            P(None, "sp", "tp"),
        ),
        out_specs=P(("grp", "sp"), "tp"),
        check_vma=False,
    )
```

time: 181 us -> 176 us (0.972)
  the two profiles are of different devices: /device:TPU:15 before, /device:TPU:24 now
where the time goes in v1:
time: 176 us
  Pallas kernels  174 us (99%)
  local copies, waits for them, and re-layouts  1.82 us (1%)
    pallas_call x1, Pallas kernels, fused(): pl.pallas_call(functools.partial(gated_conv, layers, sp, tp), out_shape=j...  174 us

profile of v1, /device:TPU:24, one launch (start us, length us, event | category | flops | bytes accessed | tf_op | source)
XLA Modules:
  0.0 175.7 jit_solution(14758354343870599708)
XLA Ops:
  0.0 173.8 %shard_map.82 = bf16[224,1024]{1,0:T(8,128)(2,1)} custom-call(bf16[224,1024]{1,0:T(8,128)(2,1)} %h_hbm.1, f32[2,4096]{1,0:T(2,128)} %gain_hbm.1, bf16[2,1024,512]{2,1,0:T(8,128)(2,1)} %wv_hbm.1, bf16[2,1024,512]{2,1,0:T(8,128)(2,1)} %wg_hbm.1, f32[31,2,512]{2,1,0:T(2,128)} %bitcast.1, f32[2,512]{1,0:T(2,128)} %lng_hbm.1, f32[2,512]{1,0:T(2,128)} %lnb_hbm.1, ...), custom_call_target="tpu_custom_call" | custom-call | tf_op jit(solution)/shard_map/pallas_call | solution.py:593
  173.8 1.8 %copy.10 = bf16[224,1024]{1,0:T(8,128)(2,1)} copy(bf16[224,1024]{1,0:T(8,128)(2,1)} %shard_map.82) | data formatting | bytes 917504

commit v2 on v1

--- a/solution.py
+++ b/solution.py
@@ -68,7 +68,7 @@
     pairs = tp // 2
     sibling = c + 1 - 2 * (c % 2)
     reach = taps_ref.shape[0]
-    pad = halo_in.shape[1]
+    pad = halo_in.shape[2]
     cuts = z_recv.shape[2]
     early = cuts // 2
     cut = share // cuts
@@ -189,11 +189,6 @@
             grp=(g + j) % grp,
         )
 
-    def z_own(l, left, k):
-        @pl.when(beyond(left) > 0)
-        def _():
-            z_copy(l, left, s, k).start()
-
     def z_pass(l, left, i, k):
         o = s + (2 * left - 1) * i
 
@@ -215,15 +210,50 @@
             for j in range(1, grp):
                 y_copy(l, j, o, g, k).start()
 
-    def z_rest(l, lean):
+    def moment(l, ahead, i, k):
+        if l == 0:
+            table = {
+                (1, 0): ("start", "start", "gathered", "gathered"),
+                (2, 0): ("start", "start", "turned", "turned"),
+                (3, 0): ("start", "start", "finished", "finished"),
+                (0, 1): ("gathered", "gathered", "summed", "summed"),
+                (1, 1): ("gathered", "gathered", "summed", "summed"),
+                (2, 1): ("summed", "finished", "counted", "counted"),
+                (0, 2): ("summed", "summed", "counted", "counted"),
+                (1, 2): ("finished", "counted", "closed", "closed"),
+            }
+        else:
+            table = {
+                (1, 0): ("start", "start", "start", "start"),
+                (2, 0): ("start", "start", "start", "start"),
+                (3, 0): ("tail", "tail", "tail", "tail"),
+                (0, 1): ("gathered", "gathered", "gathered", "gathered"),
+                (1, 1): ("before", "before", "gathered", "gathered"),
+                (2, 1): ("before", "before", "turned", "turned"),
+                (0, 2): ("summed", "summed", "summed", "summed"),
+                (1, 2): ("summed", "summed", "finished", "finished"),
+            }
+        return table.get((ahead, i), ("closed",) * 4)[4 * k // cuts]
+
+    def fill(l, point):
         for left in range(2):
-
-            @pl.when((beyond(left) <= 1) == lean)
-            def _():
-                for k in range(early if l == 0 else cuts, cuts):
-                    z_own(l, left, k)
-                for k in range(early):
-                    z_pass(l, left, 1, k)
+            for ahead in range(sp):
+                steps = [
+                    (i, k)
+                    for i in range(sp - ahead)
+                    for k in range(cuts)
+                    if moment(l, min(ahead, 3), i, k) == point
+                ]
+
+                if steps:
+
+                    @pl.when(beyond(left) == ahead)
+                    def _():
+                        for i, k in steps:
+                            if i > 0:
+                                z_pass(l, left, i, k)
+                            elif ahead > 0:
+                                z_copy(l, left, s, k).start()
 
     def place(j):
         left = (j + 2 * s // sp) % 2
@@ -268,8 +298,10 @@
             sp=s + 1 - 2 * left,
         )
 
-    def h_copy(l, to):
-        return send(halo_out.at[l], halo_in.at[l], h_send.at[l], h_recv.at[l], sp=to)
+    def h_copy(l, to, i):
+        return send(
+            halo_out.at[l, i], halo_in.at[l, i], h_send.at[l, i], h_recv.at[l, i], sp=to
+        )
 
     def s_copy(l, to, frm):
         return send(stat.at[l, frm], stat.at[l, frm], s_send.at[l, to], s_recv.at[l, frm], tp=to)
@@ -287,6 +319,8 @@
             held(d)
             b_copy(l, d, s).start()
 
+        if l > 0:
+            fill(l, "before")
         each(scatter)
         held(s)
         xs[l, c, s] = spread[l, s]
@@ -302,7 +336,7 @@
 
         gather(s)
         each(lambda j, left, d: gather(d))
-        z_rest(l, True)
+        fill(l, "gathered")
         for load in in_loads[l]:
             load.wait()
 
@@ -335,10 +369,9 @@
 
         def partial(j, left, d):
             ready(d)
-            for half, weight in enumerate((wv, wg)):
-
-                def one(i, carry):
-                    slot = half * chunks + i
+            def one(i, carry):
+                for half, weight in enumerate((wv, wg)):
+                    slot = 2 * i + half
                     own[half] = product(d, weight, pl.multiple_of(i * step, step))
 
                     @pl.when(upstream(left))
@@ -348,12 +381,16 @@
 
                     going[l, left, d, slot] = own[half].astype(BF16)
                     r_copy(l, left, d, slot).start()
-                    return carry
-
-                lax.fori_loop(0, chunks, one, 0)
+                return carry
+
+            lax.fori_loop(0, chunks, one, 0)
+
+            @pl.when(j == 0)
+            def _():
+                fill(l, "turned")
 
         each(partial)
-        z_rest(l, False)
+        fill(l, "summed")
         ready(s)
         for j in range(1, tp):
             q_copy(l, c, (c + j) % tp).wait_recv()
@@ -365,7 +402,7 @@
         def finish(i, carry):
             at = pl.multiple_of(i * step, step)
             for half, weight in enumerate((wv, wg)):
-                slot = half * chunks + i
+                slot = 2 * i + half
                 own[half] = product(s, weight, at)
                 for left in range(2):
 
@@ -376,42 +413,45 @@
 
             glu = (own[0] * scale * jax.nn.sigmoid(own[1] * scale)).astype(BF16)
             ext[pad:, pl.ds(at, step)] = glu.astype(F32)
-            halo_out[l, :, pl.ds(at, step)] = glu[rows - pad :]
+            halo_out[l, i] = glu[rows - pad :]
+
+            @pl.when(s < sp - 1)
+            def _():
+                h_copy(l, s + 1, i).start()
+
             return carry
 
         lax.fori_loop(0, chunks, finish, 0)
-
-        @pl.when(s < sp - 1)
-        def _():
-            h_copy(l, s + 1).start()
-
-        for k in range(early, cuts):
-            for left in range(2):
-                z_pass(l, left, 1, k)
-
-        @pl.when(s > 0)
-        def _():
-            h_copy(l, (s + 1) % sp).wait_recv()
-            ext[:pad] = halo_in[l].astype(F32)
-
-        @pl.when(s == 0)
-        def _():
-            ext[:pad] = jnp.zeros((pad, chans), F32)
-
         if l == 0:
             for load in small_loads:
                 load.wait()
+        fill(l, "finished")
         first = pad - (reach - 1)
 
         def convolve(i, carry):
-            lanes = pl.ds(pl.multiple_of(i * LANES, LANES), LANES)
+            at = pl.multiple_of(i * step, step)
+
+            @pl.when(s > 0)
+            def _():
+                h_copy(l, (s + 1) % sp, i).wait_recv()
+                ext[:pad, pl.ds(at, step)] = halo_in[l, i].astype(F32)
+
+            @pl.when(s == 0)
+            def _():
+                ext[:pad, pl.ds(at, step)] = jnp.zeros((pad, step), F32)
+
+            lax.fori_loop(0, step // LANES, functools.partial(strip, at), 0)
+            return carry
+
+        def strip(start, i, carry):
+            lanes = pl.ds(pl.multiple_of(start + i * LANES, LANES), LANES)
             acc = jnp.zeros((rows, LANES), F32)
             for k in range(reach):
                 acc = acc + taps_ref[k, l : l + 1, lanes] * ext[first + k : first + k + rows, lanes]
             conv[:, lanes] = acc
             return carry
 
-        lax.fori_loop(0, chans // LANES, convolve, 0)
+        lax.fori_loop(0, chunks, convolve, 0)
         total = jnp.zeros((rows, LANES), F32)
         total_sq = jnp.zeros((rows, LANES), F32)
         for at in range(0, chans, LANES):
@@ -424,9 +464,11 @@
         )
         for j in range(1, tp):
             s_copy(l, (c + j) % tp, c).start()
-        for k in range(early):
-            for left in range(2):
-                z_pass(l, left, 2, k)
+        fill(l, "counted")
+        if l + 1 < layers:
+            for load in out_loads[l + 1]:
+                load.wait()
+            fill(l + 1, "tail")
         for j in range(1, tp):
             s_copy(l, c, (c + j) % tp).wait_recv()
         stats = stat[l, 0]
@@ -446,23 +488,13 @@
         for j in range(1, pairs):
             g_copy(l, (c + 2 * j) % tp, c, g_send.at[l, j]).start()
         g_copy(l, sibling, c, g_send.at[l, 0]).start()
+        fill(l, "closed")
+        if l + 1 < layers:
+            fill(l + 1, "start")
         for j in range(1, pairs):
             p = (c + 2 * j) % tp
             g_copy(l, sibling, p, g_relay.at[l, p]).wait_recv()
             g_copy(l, sibling, p, g_relay.at[l, p]).start()
-        for k in range(early, cuts):
-            for left in range(2):
-                z_pass(l, left, 2, k)
-        for i in range(3, sp):
-            for k in range(cuts):
-                for left in range(2):
-                    z_pass(l, left, i, k)
-        if l + 1 < layers:
-            for load in out_loads[l + 1]:
-                load.wait()
-            for k in range(cuts):
-                for left in range(2):
-                    z_own(l + 1, left, k)
         for j in range(pairs):
             p = (sibling + 2 * j) % tp
             g_copy(l, sibling, p, g_relay.at[l, p]).wait_recv()
@@ -517,9 +549,7 @@
         return carry
 
     lax.fori_loop(0, tp, first_hand_out, 0)
-    for k in range(early):
-        for left in range(2):
-            z_own(0, left, k)
+    fill(0, "start")
     hand_out_squares(0)
     for l in range(layers):
         layer_of(l)
@@ -553,7 +583,8 @@
 
         @pl.when(s < sp - 1)
         def _():
-            h_copy(l, s + 1).wait_send()
+            for i in range(chunks):
+                h_copy(l, s + 1, i).wait_send()
 
         for i in range(sp):
             for left in range(2):
@@ -614,8 +645,8 @@
             vmem((layers, tp, 8, padded), F32),
             vmem((rows, LANES), F32),
             vmem((layers, tp, 8, padded), F32),
-            vmem((layers, pad, chans), BF16),
-            vmem((layers, pad, chans), BF16),
+            vmem((layers, chans // step, pad, step), BF16),
+            vmem((layers, chans // step, pad, step), BF16),
             vmem((pad + rows, chans), F32),
             vmem((rows, chans), F32),
             vmem((layers, tp, rows, chans), BF16),
@@ -624,7 +655,7 @@
             dma((layers, tp, sp)), dma((layers, tp, sp)), dma((layers, tp, sp)),
             dma((layers, 2, sp, slots)), dma((layers, 2, sp, slots)),
             dma((layers, tp)), dma((layers, tp)), dma((layers, tp)), dma((layers, tp)),
-            dma((layers,)), dma((layers,)),
+            dma((layers, chans // step)), dma((layers, chans // step)),
             dma((layers, tp)), dma((layers, tp)), dma((layers, tp)),
             dma((layers, grp)), dma((layers, 2, sp, cuts)), dma((layers, sp, cuts)),
             dma((layers, grp, sp, cuts)), dma((layers, sp, grp, cuts)),

time: 176 us -> 160 us (0.909); the launches traced: 176 us -> 157 us
  Pallas kernels: 174 us -> 156 us
    pallas_call x1, Pallas kernels: 174 us -> 156 us  [fused(): pl.pallas_call(functools.partial(gated_conv, layers, sp, tp), out_shape=j...]
where the time goes in v2:
time: 160 us; the launch traced here: 157 us
  Pallas kernels  156 us (98%)
  local copies, waits for them, and re-layouts  1.82 us (1%)
    pallas_call x1, Pallas kernels, fused(): pl.pallas_call(functools.partial(gated_conv, layers, sp, tp), out_shape=j...  156 us

profile of v2, /device:TPU:24, one launch (start us, length us, event | category | flops | bytes accessed | tf_op | source)
XLA Modules:
  0.0 157.4 jit_solution(8538100727591016114)
XLA Ops:
  0.0 155.6 %shard_map.82 = bf16[224,1024]{1,0:T(8,128)(2,1)} custom-call(bf16[224,1024]{1,0:T(8,128)(2,1)} %h_hbm.1, f32[2,4096]{1,0:T(2,128)} %gain_hbm.1, bf16[2,1024,512]{2,1,0:T(8,128)(2,1)} %wv_hbm.1, bf16[2,1024,512]{2,1,0:T(8,128)(2,1)} %wg_hbm.1, f32[31,2,512]{2,1,0:T(2,128)} %bitcast.1, f32[2,512]{1,0:T(2,128)} %lng_hbm.1, f32[2,512]{1,0:T(2,128)} %lnb_hbm.1, ...), custom_call_target="tpu_custom_call" | custom-call | tf_op jit(solution)/shard_map/pallas_call | solution.py:624
  155.6 1.8 %copy.10 = bf16[224,1024]{1,0:T(8,128)(2,1)} copy(bf16[224,1024]{1,0:T(8,128)(2,1)} %shard_map.82) | data formatting | bytes 917504

commit v3 on v2

--- a/solution.py
+++ b/solution.py
@@ -9,7 +9,29 @@
 
 LANES = 128
 BF16, F32 = jnp.bfloat16, jnp.float32
+LOTS = 2
 CUTS = 4
+
+FIRST = {
+    (1, 0): ("start", "start", "gathered", "gathered"),
+    (2, 0): ("start", "start", "scattered", "turned"),
+    (3, 0): ("start", "start", "scattered", "finished"),
+    (0, 1): ("gathered", "gathered", "summed", "summed"),
+    (1, 1): ("gathered", "gathered", "summed", "summed"),
+    (2, 1): ("gathered summed", "gathered finished", "gathered finished", "counted"),
+    (0, 2): ("summed", "summed", "counted", "counted"),
+    (1, 2): ("counted", "counted", "closed", "closed"),
+}
+LATER = {
+    (1, 0): ("start", "start", "start", "start"),
+    (2, 0): ("tail", "tail", "tail", "tail"),
+    (3, 0): ("tail", "tail", "tail", "tail"),
+    (0, 1): ("gathered", "gathered", "gathered", "gathered"),
+    (1, 1): ("gathered", "gathered", "gathered", "gathered"),
+    (2, 1): ("start", "before", "scattered", "finished"),
+    (0, 2): ("summed", "summed", "summed", "summed"),
+    (1, 2): ("summed", "summed", "counted", "counted"),
+}
 
 
 def passed_along(block, axis, distance):
@@ -51,11 +73,11 @@
     layers, sp, tp,
     h_hbm, gain_hbm, wv_hbm, wg_hbm, taps_hbm, lng_hbm, lnb_hbm, wo_hbm, out_ref,
     h_ref, gain_ref, taps_ref, lng_ref, lnb_ref, mid,
-    wv, wg, wo, pieces, spread, xs, going, coming, own, sq, sq_sum, stat,
+    wvg, wo, lent, pieces, spread, xs, going, coming, own, sq, sq_sum, stat,
     halo_out, halo_in, ext, conv, acts,
     i_sem, w_sem, a_send, a_recv, b_send, c_send, c_relay, x_recv, r_send, r_recv,
     q_send, q_recv, s_send, s_recv, h_send, h_recv, g_send, g_relay, g_recv,
-    o_sem, z_send, z_recv, y_send, y_recv,
+    o_sem, z_send, z_recv, y_send, y_recv, v_send, v_recv, u_send, u_recv,
 ):
     s, c, g = lax.axis_index("sp"), lax.axis_index("tp"), lax.axis_index("grp")
     grp, share = wo.shape[2], wo.shape[3]
@@ -72,6 +94,13 @@
     cuts = z_recv.shape[2]
     early = cuts // 2
     cut = share // cuts
+    lots = v_recv.shape[2]
+    lot = depth // (grp * lots)
+    early_lots = 2 * lots
+    kept = chunks - lent.shape[3] // step
+    at_end = (s == 0) | (s == sp - 1)
+    at_host = (s == 1) | (s == sp - 2)
+    partner = (s == 0) + (sp - 2) * (s == sp - 1) + (sp - 1) * (s == sp - 2)
 
     first_loads = [
         pltpu.make_async_copy(h_hbm, h_ref, i_sem.at[0]),
@@ -86,8 +115,8 @@
     ]
     in_loads = [
         (
-            pltpu.make_async_copy(wv_hbm.at[l], wv.at[l], w_sem.at[l, 0]),
-            pltpu.make_async_copy(wg_hbm.at[l], wg.at[l], w_sem.at[l, 1]),
+            pltpu.make_async_copy(wv_hbm.at[l], wvg.at[l, 0], w_sem.at[l, 0]),
+            pltpu.make_async_copy(wg_hbm.at[l], wvg.at[l, 1], w_sem.at[l, 1]),
         )
         for l in range(layers)
     ]
@@ -189,71 +218,96 @@
             grp=(g + j) % grp,
         )
 
-    def z_pass(l, left, i, k):
-        o = s + (2 * left - 1) * i
-
-        @pl.when((o >= 0) & (o < sp))
-        def _():
-            rows_k = pl.ds(k * cut, cut)
-            send(
-                wo.at[l, o, g, rows_k],
-                wo.at[l, o, g, rows_k],
-                z_send.at[l, left, o, k],
-                z_recv.at[l, o, k],
-                sp=(s + 1) % sp,
-            ).wait_recv()
-
-            @pl.when(beyond(left) > 0)
-            def _():
-                z_copy(l, left, o, k).start()
-
-            for j in range(1, grp):
-                y_copy(l, j, o, g, k).start()
+    def z_take(l, o, k):
+        rows_k = pl.ds(k * cut, cut)
+        send(
+            wo.at[l, o, g, rows_k],
+            wo.at[l, o, g, rows_k],
+            z_send.at[l, 0, o, k],
+            z_recv.at[l, o, k],
+            sp=(s + 1) % sp,
+        ).wait_recv()
+        for j in range(1, grp):
+            y_copy(l, j, o, g, k).start()
 
     def moment(l, ahead, i, k):
         if l == 0:
-            table = {
-                (1, 0): ("start", "start", "gathered", "gathered"),
-                (2, 0): ("start", "start", "turned", "turned"),
-                (3, 0): ("start", "start", "finished", "finished"),
-                (0, 1): ("gathered", "gathered", "summed", "summed"),
-                (1, 1): ("gathered", "gathered", "summed", "summed"),
-                (2, 1): ("summed", "finished", "counted", "counted"),
-                (0, 2): ("summed", "summed", "counted", "counted"),
-                (1, 2): ("finished", "counted", "closed", "closed"),
-            }
+            table = FIRST
         else:
-            table = {
-                (1, 0): ("start", "start", "start", "start"),
-                (2, 0): ("start", "start", "start", "start"),
-                (3, 0): ("tail", "tail", "tail", "tail"),
-                (0, 1): ("gathered", "gathered", "gathered", "gathered"),
-                (1, 1): ("before", "before", "gathered", "gathered"),
-                (2, 1): ("before", "before", "turned", "turned"),
-                (0, 2): ("summed", "summed", "summed", "summed"),
-                (1, 2): ("summed", "summed", "finished", "finished"),
-            }
-        return table.get((ahead, i), ("closed",) * 4)[4 * k // cuts]
+            table = LATER
+        points = table.get((ahead, i), ("closed",) * 4)[4 * k // cuts]
+        return points.split() if " " in points else (points, points)
 
     def fill(l, point):
         for left in range(2):
             for ahead in range(sp):
-                steps = [
-                    (i, k)
-                    for i in range(sp - ahead)
-                    for k in range(cuts)
-                    if moment(l, min(ahead, 3), i, k) == point
-                ]
+                steps = []
+                for i in range(sp - ahead):
+                    for k in range(cuts):
+                        taken, sent_on = moment(l, min(ahead, 3), i, k)
+                        if i > 0 and taken == point:
+                            steps.append((i, k, True))
+                        if ahead > 0 and sent_on == point:
+                            steps.append((i, k, False))
 
                 if steps:
 
                     @pl.when(beyond(left) == ahead)
                     def _():
-                        for i, k in steps:
-                            if i > 0:
-                                z_pass(l, left, i, k)
-                            elif ahead > 0:
-                                z_copy(l, left, s, k).start()
+                        for i, k, take in steps:
+                            o = s + (2 * left - 1) * i
+                            if take:
+                                z_take(l, o, k)
+                            else:
+                                z_copy(l, left, o, k).start()
+
+    def lends(l):
+        return l > 0 and sp >= 4 and kept < chunks
+
+    def sent_chunks(l, d):
+        if not lends(l):
+            return chunks
+        return chunks - (chunks - kept) * (at_end & (d == partner)).astype(jnp.int32)
+
+    def v_copy(l, t):
+        half, q = t % 2, t // 2
+        rows_q = pl.ds(pl.multiple_of((g * lots + q) * lot, lot), lot)
+        return send(
+            wvg.at[l, half, rows_q, pl.ds(kept * step, (chunks - kept) * step)],
+            lent.at[l - 1, half, rows_q],
+            v_send.at[l - 1, half, q],
+            v_recv.at[l - 1, half, q],
+            sp=partner,
+        )
+
+    def u_copy(l, j, t, n):
+        half, q = t % 2, t // 2
+        rows_q = pl.ds(pl.multiple_of((n * lots + q) * lot, lot), lot)
+        return send(
+            lent.at[l - 1, half, rows_q],
+            lent.at[l - 1, half, rows_q],
+            u_send.at[l - 1, j, half, q],
+            u_recv.at[l - 1, half, n, q],
+            grp=(g + j) % grp,
+        )
+
+    def lend_out(l, first, last):
+        if lends(l):
+
+            @pl.when(at_end)
+            def _():
+                for t in range(first, last):
+                    v_copy(l, t).start()
+
+    def lend_in(l, first, last):
+        if lends(l):
+
+            @pl.when(at_host)
+            def _():
+                for t in range(first, last):
+                    v_copy(l, t).wait_recv()
+                    for j in range(1, grp):
+                        u_copy(l, j, t, g).start()
 
     def place(j):
         left = (j + 2 * s // sp) % 2
@@ -273,8 +327,11 @@
 
         lax.fori_loop(0, 2 * (sp - 1), one, 0)
 
+    def behind(left):
+        return (1 - left) * s + left * (sp - 1 - s)
+
     def upstream(left):
-        return (1 - left) * s + left * (sp - 1 - s) > 0
+        return behind(left) > 0
 
     def b_copy(l, to, frm):
         return send(
@@ -310,6 +367,10 @@
         return send(acts.at[l, p], acts.at[l, p], sem, g_recv.at[l, p], tp=to)
 
     def layer_of(l):
+        slots = 2 * chunks
+        inner = sp == 4 and slots >= 2
+        mids = 1 - at_end.astype(jnp.int32)
+
         def held(e):
             @pl.when(e != c)
             def _():
@@ -321,24 +382,33 @@
 
         if l > 0:
             fill(l, "before")
+            lend_in(l, 0, lots)
         each(scatter)
+        fill(l, "scattered")
         held(s)
         xs[l, c, s] = spread[l, s]
-
-        def gather(d):
-            @pl.when(d != s)
-            def _():
+        if lends(l):
+
+            @pl.when(at_host)
+            def _():
+                xs[l, c, sp] = spread[l, partner]
+
+        def gather(d, arriving=True):
+            if arriving:
                 relay(l, c, d).wait_recv()
-
             for j in range(1, pairs):
                 c_copy(l, (c + 2 * j) % tp, d, c_send.at[l, j, d]).start()
             c_copy(l, sibling, d, c_send.at[l, 0, d]).start()
 
-        gather(s)
-        each(lambda j, left, d: gather(d))
-        fill(l, "gathered")
-        for load in in_loads[l]:
-            load.wait()
+        gather(s, False)
+        if inner:
+            gather(place(0)[1])
+            gather(place(1 + at_end.astype(jnp.int32))[1])
+        else:
+            each(lambda j, left, d: gather(d))
+        if l == 0:
+            for load in in_loads[l]:
+                load.wait()
 
         def ready(d):
             for j in range(1, pairs):
@@ -353,7 +423,7 @@
             for p in range(tp):
                 acc = acc + jnp.dot(
                     xs[l, p, d],
-                    weight[l, p * part : (p + 1) * part, pl.ds(at, step)],
+                    weight[p * part : (p + 1) * part, pl.ds(at, step)],
                     preferred_element_type=F32,
                 )
             return acc
@@ -367,31 +437,79 @@
                 sp=(s + 1) % sp,
             ).wait_recv()
 
-        def partial(j, left, d):
-            ready(d)
-            def one(i, carry):
-                for half, weight in enumerate((wv, wg)):
-                    slot = 2 * i + half
-                    own[half] = product(d, weight, pl.multiple_of(i * step, step))
-
-                    @pl.when(upstream(left))
+        def partial(slot, left, d):
+            half, i = slot % 2, slot // 2
+
+            @pl.when(slot == 0)
+            def _():
+                ready(d)
+
+            own[half] = product(d, wvg.at[l, half], pl.multiple_of(i * step, step))
+
+            @pl.when(upstream(left))
+            def _():
+                r_arrived(left, d, slot)
+                own[half] += coming[l, left, d, slot].astype(F32)
+
+            going[l, left, d, slot] = own[half].astype(BF16)
+            r_copy(l, left, d, slot).start()
+
+        def turn_slot(t):
+            if not inner:
+                return t // slots, t % slots
+            u = t - 2
+            woven = ((u >= 0) & (u < 2 * slots)).astype(jnp.int32)
+            aside = woven * (1 - u % 2) * mids
+            k = jnp.where(woven == 1, 2 + u // 2, jnp.where(u < 0, t, t - slots))
+            k = mids * k + (1 - mids) * t
+            j = aside + (1 - aside) * 2 * (k // slots)
+            return j, aside * (u // 2) + (1 - aside) * (k % slots)
+
+        def advance(t, carry):
+            j, slot = turn_slot(t)
+            left, d, valid = place(j)
+
+            @pl.when(valid & (slot < 2 * sent_chunks(l, d)))
+            def _():
+                partial(slot, left, d)
+
+            @pl.when(t == 0)
+            def _():
+                if inner:
+                    gather(place(2 + 2 * at_end.astype(jnp.int32))[1])
+                if lends(l):
+
+                    @pl.when(at_host)
                     def _():
-                        r_arrived(left, d, slot)
-                        own[half] += coming[l, left, d, slot].astype(F32)
-
-                    going[l, left, d, slot] = own[half].astype(BF16)
-                    r_copy(l, left, d, slot).start()
-                return carry
-
-            lax.fori_loop(0, chunks, one, 0)
-
-            @pl.when(j == 0)
+                        gather(sp, False)
+
+                lend_in(l, lots, early_lots)
+                fill(l, "gathered")
+                lend_out(l, early_lots, 2 * lots)
+
+            @pl.when(t == slots - 1 + (mids * (slots - 2) if inner else 0))
             def _():
                 fill(l, "turned")
-
-        each(partial)
+                lend_in(l, early_lots, 2 * lots)
+
+            @pl.when(t == 2 * slots - 1)
+            def _():
+                fill(l, "halfway")
+
+            return carry
+
+        lax.fori_loop(0, slots * (3 if inner else 2 * (sp - 1)), advance, 0)
         fill(l, "summed")
         ready(s)
+        if lends(l):
+
+            @pl.when(at_host)
+            def _():
+                ready(sp)
+                for t in range(2 * lots):
+                    for j in range(1, grp):
+                        u_copy(l, j, t, (g + j) % grp).wait_recv()
+
         for j in range(1, tp):
             q_copy(l, c, (c + j) % tp).wait_recv()
         squares = sq[l, 0]
@@ -401,12 +519,25 @@
 
         def finish(i, carry):
             at = pl.multiple_of(i * step, step)
-            for half, weight in enumerate((wv, wg)):
+            for half in range(2):
                 slot = 2 * i + half
-                own[half] = product(s, weight, at)
+                own[half] = product(s, wvg.at[l, half], at)
+                if lends(l):
+
+                    @pl.when(at_host & (i >= kept))
+                    def _():
+                        own[half] += product(
+                            sp, lent.at[l - 1, half], pl.multiple_of(at - kept * step, step)
+                        )
+
                 for left in range(2):
-
-                    @pl.when(upstream(left))
+                    expected = upstream(left)
+                    if lends(l):
+                        expected = expected & jnp.logical_not(
+                            at_host & (behind(left) == 1) & (i >= kept)
+                        )
+
+                    @pl.when(expected)
                     def _():
                         r_arrived(left, s, slot)
                         own[half] += coming[l, left, s, slot].astype(F32)
@@ -468,7 +599,10 @@
         if l + 1 < layers:
             for load in out_loads[l + 1]:
                 load.wait()
+            for load in in_loads[l + 1]:
+                load.wait()
             fill(l + 1, "tail")
+            lend_out(l + 1, 0, early_lots)
         for j in range(1, tp):
             s_copy(l, c, (c + j) % tp).wait_recv()
         stats = stat[l, 0]
@@ -559,25 +693,38 @@
             a_copy(l, (c + j) % tp, c).wait_send()
             q_copy(l, (c + j) % tp, c).wait_send()
             s_copy(l, (c + j) % tp, c).wait_send()
-        for j in range(1, sp):
-            b_copy(l, (s + j) % sp, s).wait_send()
-
-        def sent(d, carry):
+        each(lambda j, left, d: b_copy(l, d, s).wait_send())
+
+        def sent(d):
             c_copy(l, sibling, d, c_send.at[l, 0, d]).wait_send()
             for j in range(1, pairs):
                 p = (c + 2 * j) % tp
                 c_copy(l, p, d, c_send.at[l, j, d]).wait_send()
                 relay(l, p, d).wait_send()
-            return carry
-
-        lax.fori_loop(0, sp, sent, 0)
+
+        sent(s)
+        each(lambda j, left, d: sent(d))
+        if lends(l):
+
+            @pl.when(at_host)
+            def _():
+                sent(sp)
+                for t in range(2 * lots):
+                    for j in range(1, grp):
+                        u_copy(l, j, t, g).wait_send()
+
+            @pl.when(at_end)
+            def _():
+                for t in range(2 * lots):
+                    v_copy(l, t).wait_send()
+
 
         def partial_sent(j, left, d):
             def one(slot, carry):
                 r_copy(l, left, d, slot).wait_send()
                 return carry
 
-            lax.fori_loop(0, 2 * chunks, one, 0)
+            lax.fori_loop(0, 2 * sent_chunks(l, d), one, 0)
 
         each(partial_sent)
 
@@ -633,12 +780,12 @@
             vmem((layers, chans), F32),
             vmem((layers, chans), F32),
             vmem((layers, rows, depth), BF16),
-            vmem((layers, depth, chans), BF16),
-            vmem((layers, depth, chans), BF16),
+            vmem((layers, 2, depth, chans), BF16),
             vmem((layers, sp, grp, share, depth), BF16),
+            vmem((max(layers - 1, 1), 2, depth, chans // step // 2 * step), BF16),
             vmem((layers, tp, rows, part), BF16),
             vmem((layers, tp, rows, part), BF16),
-            vmem((layers, tp, sp, rows, part), BF16),
+            vmem((layers, tp, sp + 1, rows, part), BF16),
             vmem((layers, 2, sp, slots, rows, step), BF16),
             vmem((layers, 2, sp, slots, rows, step), BF16),
             vmem((2, rows, step), F32),
@@ -652,13 +799,15 @@
             vmem((layers, tp, rows, chans), BF16),
             dma((5,)), dma((layers, 2)),
             dma((layers, tp)), dma((layers, tp)), dma((layers, sp)),
-            dma((layers, tp, sp)), dma((layers, tp, sp)), dma((layers, tp, sp)),
+            dma((layers, tp, sp + 1)), dma((layers, tp, sp + 1)), dma((layers, tp, sp + 1)),
             dma((layers, 2, sp, slots)), dma((layers, 2, sp, slots)),
             dma((layers, tp)), dma((layers, tp)), dma((layers, tp)), dma((layers, tp)),
             dma((layers, chans // step)), dma((layers, chans // step)),
             dma((layers, tp)), dma((layers, tp)), dma((layers, tp)),
             dma((layers, grp)), dma((layers, 2, sp, cuts)), dma((layers, sp, cuts)),
             dma((layers, grp, sp, cuts)), dma((layers, sp, grp, cuts)),
+            dma((layers, 2, LOTS)), dma((layers, 2, LOTS)),
+            dma((layers, grp, 2, LOTS)), dma((layers, 2, grp, LOTS)),
         ],
         compiler_params=pltpu.CompilerParams(
             collective_id=0, has_side_effects=True, vmem_limit_bytes=60 * 2**20
@@ -679,6 +828,7 @@
         and chans % (LANES * grp) == 0
         and w_out.shape[1] % (16 * grp * CUTS) == 0
         and w_out.shape[1] == chans
+        and depth % (16 * grp * LOTS) == 0
         and chans % min(2 * LANES, chans) == 0
         and rows % 16 == 0
         and rows >= -(-(taps.shape[1] - 1) // 16) * 16

time: 160 us -> 152 us (0.950)
  Pallas kernels: 156 us -> 149 us
    pallas_call x1, Pallas kernels: 156 us -> 149 us  [fused(): pl.pallas_call(functools.partial(gated_conv, layers, sp, tp), out_shape=j...]
where the time goes in v3:
time: 152 us; the launch traced here: 151 us
  Pallas kernels  149 us (98%)
  local copies, waits for them, and re-layouts  1.82 us (1%)
    pallas_call x1, Pallas kernels, fused(): pl.pallas_call(functools.partial(gated_conv, layers, sp, tp), out_shape=j...  149 us

profile of v3, /device:TPU:24, one launch (start us, length us, event | category | flops | bytes accessed | tf_op | source)
XLA Modules:
  0.0 150.5 jit_solution(10204583775155366556)
XLA Ops:
  0.0 148.7 %shard_map.82 = bf16[224,1024]{1,0:T(8,128)(2,1)} custom-call(bf16[224,1024]{1,0:T(8,128)(2,1)} %h_hbm.1, f32[2,4096]{1,0:T(2,128)} %gain_hbm.1, bf16[2,1024,512]{2,1,0:T(8,128)(2,1)} %wv_hbm.1, bf16[2,1024,512]{2,1,0:T(8,128)(2,1)} %wg_hbm.1, f32[31,2,512]{2,1,0:T(2,128)} %bitcast.1, f32[2,512]{1,0:T(2,128)} %lng_hbm.1, f32[2,512]{1,0:T(2,128)} %lnb_hbm.1, ...), custom_call_target="tpu_custom_call" | custom-call | tf_op jit(solution)/shard_map/pallas_call | solution.py:771
  148.7 1.8 %copy.10 = bf16[224,1024]{1,0:T(8,128)(2,1)} copy(bf16[224,1024]{1,0:T(8,128)(2,1)} %shard_map.82) | data formatting | bytes 917504

commit v4 on v3

--- a/solution.py
+++ b/solution.py
@@ -10,7 +10,7 @@
 LANES = 128
 BF16, F32 = jnp.bfloat16, jnp.float32
 LOTS = 2
-CUTS = 4
+CUTS = 8
 
 FIRST = {
     (1, 0): ("start", "start", "gathered", "gathered"),
@@ -27,10 +27,11 @@
     (2, 0): ("tail", "tail", "tail", "tail"),
     (3, 0): ("tail", "tail", "tail", "tail"),
     (0, 1): ("gathered", "gathered", "gathered", "gathered"),
-    (1, 1): ("gathered", "gathered", "gathered", "gathered"),
+    (1, 1): ("before", "before", "gathered", "gathered"),
     (2, 1): ("start", "before", "scattered", "finished"),
     (0, 2): ("summed", "summed", "summed", "summed"),
     (1, 2): ("summed", "summed", "counted", "counted"),
+    (0, 3): ("counted", "counted", "closed", "closed"),
 }
 
 
@@ -76,7 +77,7 @@
     wvg, wo, lent, pieces, spread, xs, going, coming, own, sq, sq_sum, stat,
     halo_out, halo_in, ext, conv, acts,
     i_sem, w_sem, a_send, a_recv, b_send, c_send, c_relay, x_recv, r_send, r_recv,
-    q_send, q_recv, s_send, s_recv, h_send, h_recv, g_send, g_relay, g_recv,
+    q_send, q_recv, s_send, s_recv, h_send, h_recv, g_send, g_recv,
     o_sem, z_send, z_recv, y_send, y_recv, v_send, v_recv, u_send, u_recv,
 ):
     s, c, g = lax.axis_index("sp"), lax.axis_index("tp"), lax.axis_index("grp")
@@ -94,6 +95,8 @@
     cuts = z_recv.shape[2]
     early = cuts // 2
     cut = share // cuts
+    bands = stat.shape[1]
+    band = rows // bands
     lots = v_recv.shape[2]
     lot = depth // (grp * lots)
     early_lots = 2 * lots
@@ -154,22 +157,26 @@
         )
 
     def to_row(column):
-        column = jnp.concatenate([column, jnp.zeros((padded - rows, LANES), F32)], axis=0)
+        blank = -column.shape[0] % LANES
+        column = jnp.concatenate([column, jnp.zeros((blank, LANES), F32)], axis=0)
         return jnp.sum(column.T, axis=0, keepdims=True)
 
-    def to_column(row):
-        return jnp.broadcast_to(row, (LANES, padded)).T[:rows, 0:1]
+    def to_column(row, size):
+        return jnp.broadcast_to(row, (LANES, row.shape[1])).T[:size, 0:1]
+
+    def all_of(block, sem):
+        return send(block, block, sem, sem, tp=sibling)
 
     def turn(i):
         return ((c // 2 + 1 + i // 2) % pairs) * 2 + (c + 1 + i) % 2
 
     def a_copy(l, to, frm):
         return send(
-            pieces.at[l, to], spread.at[l, frm], a_send.at[l, to], a_recv.at[l, frm], tp=to
+            pieces.at[l, to], spread.at[l, frm], a_send.at[l], a_recv.at[l, frm], tp=to
         )
 
     def q_copy(l, to, frm):
-        return send(sq.at[l, frm], sq.at[l, frm], q_send.at[l, to], q_recv.at[l, frm], tp=to)
+        return send(sq.at[l, frm], sq.at[l, frm], q_send.at[l], q_recv.at[l], tp=to)
 
     def prepare(l, p, block):
         wide = block.astype(F32)
@@ -203,7 +210,7 @@
         return send(
             wo.at[l, o, g, rows_k],
             wo.at[l, o, g, rows_k],
-            z_send.at[l, left, o, k],
+            z_send.at[l, left],
             z_recv.at[l, o, k],
             sp=s + 1 - 2 * left,
         )
@@ -213,8 +220,8 @@
         return send(
             wo.at[l, o, n, rows_k],
             wo.at[l, o, n, rows_k],
-            y_send.at[l, j, o, k],
-            y_recv.at[l, o, n, k],
+            y_send.at[l, j],
+            y_recv.at[l, n],
             grp=(g + j) % grp,
         )
 
@@ -223,7 +230,7 @@
         send(
             wo.at[l, o, g, rows_k],
             wo.at[l, o, g, rows_k],
-            z_send.at[l, 0, o, k],
+            z_send.at[l, 0],
             z_recv.at[l, o, k],
             sp=(s + 1) % sp,
         ).wait_recv()
@@ -275,7 +282,7 @@
         return send(
             wvg.at[l, half, rows_q, pl.ds(kept * step, (chunks - kept) * step)],
             lent.at[l - 1, half, rows_q],
-            v_send.at[l - 1, half, q],
+            v_send.at[l - 1],
             v_recv.at[l - 1, half, q],
             sp=partner,
         )
@@ -286,10 +293,13 @@
         return send(
             lent.at[l - 1, half, rows_q],
             lent.at[l - 1, half, rows_q],
-            u_send.at[l - 1, j, half, q],
-            u_recv.at[l - 1, half, n, q],
+            u_send.at[l - 1, j],
+            u_recv.at[l - 1, n],
             grp=(g + j) % grp,
         )
+
+    def lot_of(l):
+        return lent.at[l - 1, pl.ds(0, 2), pl.ds(0, depth // grp)]
 
     def lend_out(l, first, last):
         if lends(l):
@@ -335,7 +345,7 @@
 
     def b_copy(l, to, frm):
         return send(
-            spread.at[l, to], xs.at[l, c, frm], b_send.at[l, to], x_recv.at[l, c, frm], sp=to
+            spread.at[l, to], xs.at[l, c, frm], b_send.at[l], x_recv.at[l, c, frm], sp=to
         )
 
     def c_copy(l, to, d, sem):
@@ -343,14 +353,14 @@
 
     def relay(l, p, d):
         return send(
-            xs.at[l, p, d], xs.at[l, p, d], c_relay.at[l, p, d], x_recv.at[l, p, d], tp=sibling
+            xs.at[l, p, d], xs.at[l, p, d], c_relay.at[l, p], x_recv.at[l, p, d], tp=sibling
         )
 
     def r_copy(l, left, d, slot):
         return send(
             going.at[l, left, d, slot],
             coming.at[l, left, d, slot],
-            r_send.at[l, left, d, slot],
+            r_send.at[l, left, slot],
             r_recv.at[l, left, d, slot],
             sp=s + 1 - 2 * left,
         )
@@ -360,11 +370,14 @@
             halo_out.at[l, i], halo_in.at[l, i], h_send.at[l, i], h_recv.at[l, i], sp=to
         )
 
-    def s_copy(l, to, frm):
-        return send(stat.at[l, frm], stat.at[l, frm], s_send.at[l, to], s_recv.at[l, frm], tp=to)
-
-    def g_copy(l, to, p, sem):
-        return send(acts.at[l, p], acts.at[l, p], sem, g_recv.at[l, p], tp=to)
+    def s_copy(l, b, to, frm):
+        return send(
+            stat.at[l, b, frm], stat.at[l, b, frm], s_send.at[l, b], s_recv.at[l, b], tp=to
+        )
+
+    def g_copy(l, b, to, p):
+        block = acts.at[l, p, pl.ds(b * band, band)]
+        return send(block, block, g_send.at[l, b], g_recv.at[l, p, b], tp=to)
 
     def layer_of(l):
         slots = 2 * chunks
@@ -397,8 +410,8 @@
             if arriving:
                 relay(l, c, d).wait_recv()
             for j in range(1, pairs):
-                c_copy(l, (c + 2 * j) % tp, d, c_send.at[l, j, d]).start()
-            c_copy(l, sibling, d, c_send.at[l, 0, d]).start()
+                c_copy(l, (c + 2 * j) % tp, d, c_send.at[l, j]).start()
+            c_copy(l, sibling, d, c_send.at[l, 0]).start()
 
         gather(s, False)
         if inner:
@@ -432,7 +445,7 @@
             send(
                 going.at[l, left, d, slot],
                 coming.at[l, left, d, slot],
-                r_send.at[l, left, d, slot],
+                r_send.at[l, left, slot],
                 r_recv.at[l, left, d, slot],
                 sp=(s + 1) % sp,
             ).wait_recv()
@@ -506,16 +519,14 @@
             @pl.when(at_host)
             def _():
                 ready(sp)
-                for t in range(2 * lots):
-                    for j in range(1, grp):
-                        u_copy(l, j, t, (g + j) % grp).wait_recv()
-
-        for j in range(1, tp):
-            q_copy(l, c, (c + j) % tp).wait_recv()
+                for j in range(1, grp):
+                    all_of(lot_of(l), u_recv.at[l - 1, (g + j) % grp]).wait_recv()
+
+        all_of(sq.at[l, pl.ds(0, tp - 1)], q_recv.at[l]).wait_recv()
         squares = sq[l, 0]
         for p in range(1, tp):
             squares = squares + sq[l, p]
-        scale = to_column(lax.rsqrt(squares[0:1] / (depth * tp) + 1e-06))
+        scale = to_column(lax.rsqrt(squares[0:1] / (depth * tp) + 1e-06), rows)
 
         def finish(i, carry):
             at = pl.multiple_of(i * step, step)
@@ -559,42 +570,49 @@
         fill(l, "finished")
         first = pad - (reach - 1)
 
-        def convolve(i, carry):
-            at = pl.multiple_of(i * step, step)
+        def halo_in_place(i, carry):
+            lanes = pl.ds(pl.multiple_of(i * step, step), step)
 
             @pl.when(s > 0)
             def _():
                 h_copy(l, (s + 1) % sp, i).wait_recv()
-                ext[:pad, pl.ds(at, step)] = halo_in[l, i].astype(F32)
+                ext[:pad, lanes] = halo_in[l, i].astype(F32)
 
             @pl.when(s == 0)
             def _():
-                ext[:pad, pl.ds(at, step)] = jnp.zeros((pad, step), F32)
-
-            lax.fori_loop(0, step // LANES, functools.partial(strip, at), 0)
+                ext[:pad, lanes] = jnp.zeros((pad, step), F32)
+
             return carry
 
-        def strip(start, i, carry):
-            lanes = pl.ds(pl.multiple_of(start + i * LANES, LANES), LANES)
-            acc = jnp.zeros((rows, LANES), F32)
+        def strip(b, i, carry):
+            lanes = pl.ds(pl.multiple_of(i * LANES, LANES), LANES)
+            above = first + b * band
+            acc = jnp.zeros((band, LANES), F32)
             for k in range(reach):
-                acc = acc + taps_ref[k, l : l + 1, lanes] * ext[first + k : first + k + rows, lanes]
-            conv[:, lanes] = acc
+                acc = acc + taps_ref[k, l : l + 1, lanes] * ext[above + k : above + k + band, lanes]
+            conv[b * band : (b + 1) * band, lanes] = acc
             return carry
 
-        lax.fori_loop(0, chunks, convolve, 0)
-        total = jnp.zeros((rows, LANES), F32)
-        total_sq = jnp.zeros((rows, LANES), F32)
-        for at in range(0, chans, LANES):
-            tile = conv[:, at : at + LANES]
-            total = total + tile
-            total_sq = total_sq + tile * tile
-        half = sq.shape[2] // 2
-        stat[l, c] = jnp.concatenate(
-            [jnp.broadcast_to(to_row(t), (half, padded)) for t in (total, total_sq)], axis=0
-        )
-        for j in range(1, tp):
-            s_copy(l, (c + j) % tp, c).start()
+        half = stat.shape[3] // 2
+        for b in reversed(range(bands)):
+            if b == 0:
+                lax.fori_loop(0, chunks, halo_in_place, 0)
+            lax.fori_loop(0, chans // LANES, functools.partial(strip, b), 0)
+            total = jnp.zeros((band, LANES), F32)
+            total_sq = jnp.zeros((band, LANES), F32)
+            for at in range(0, chans, LANES):
+                tile = conv[b * band : (b + 1) * band, at : at + LANES]
+                total = total + tile
+                total_sq = total_sq + tile * tile
+            stat[l, b, c] = jnp.concatenate(
+                [
+                    jnp.broadcast_to(to_row(t), (half, stat.shape[4]))
+                    for t in (total, total_sq)
+                ],
+                axis=0,
+            )
+            for j in range(1, tp):
+                s_copy(l, b, (c + j) % tp, c).start()
         fill(l, "counted")
         if l + 1 < layers:
             for load in out_loads[l + 1]:
@@ -603,44 +621,39 @@
                 load.wait()
             fill(l + 1, "tail")
             lend_out(l + 1, 0, early_lots)
-        for j in range(1, tp):
-            s_copy(l, c, (c + j) % tp).wait_recv()
-        stats = stat[l, 0]
-        for p in range(1, tp):
-            stats = stats + stat[l, p]
-        mean = stats[0:1] / (chans * tp)
-        var = stats[half : half + 1] / (chans * tp) - mean * mean
-        inv = to_column(lax.rsqrt(var + 1e-05))
-        mean = to_column(mean)
-        for at in range(0, chans, LANES):
-            lanes = slice(at, at + LANES)
-            shaped = (conv[:, lanes] - mean) * inv * lng_ref[l : l + 1, lanes] + lnb_ref[
-                l : l + 1, lanes
-            ]
-            acts[l, c, :, lanes] = (shaped / (1.0 + jnp.exp(-shaped))).astype(BF16)
-
-        for j in range(1, pairs):
-            g_copy(l, (c + 2 * j) % tp, c, g_send.at[l, j]).start()
-        g_copy(l, sibling, c, g_send.at[l, 0]).start()
+        for b in reversed(range(bands)):
+            all_of(stat.at[l, b, pl.ds(0, tp - 1)], s_recv.at[l, b]).wait_recv()
+            stats = stat[l, b, 0]
+            for p in range(1, tp):
+                stats = stats + stat[l, b, p]
+            mean = stats[0:1] / (chans * tp)
+            var = stats[half : half + 1] / (chans * tp) - mean * mean
+            inv = to_column(lax.rsqrt(var + 1e-05), band)
+            mean = to_column(mean, band)
+            here = slice(b * band, (b + 1) * band)
+            for at in range(0, chans, LANES):
+                lanes = slice(at, at + LANES)
+                shaped = (conv[here, lanes] - mean) * inv * lng_ref[l : l + 1, lanes] + lnb_ref[
+                    l : l + 1, lanes
+                ]
+                acts[l, c, here, lanes] = (shaped / (1.0 + jnp.exp(-shaped))).astype(BF16)
+            for j in range(1, pairs):
+                g_copy(l, b, (c + 2 * j) % tp, c).start()
+            g_copy(l, b, sibling, c).start()
         fill(l, "closed")
         if l + 1 < layers:
             fill(l + 1, "start")
-        for j in range(1, pairs):
-            p = (c + 2 * j) % tp
-            g_copy(l, sibling, p, g_relay.at[l, p]).wait_recv()
-            g_copy(l, sibling, p, g_relay.at[l, p]).start()
+        for b in reversed(range(bands)):
+            for j in range(1, pairs):
+                p = (c + 2 * j) % tp
+                g_copy(l, b, sibling, p).wait_recv()
+                g_copy(l, b, sibling, p).start()
         for j in range(pairs):
             p = (sibling + 2 * j) % tp
-            g_copy(l, sibling, p, g_relay.at[l, p]).wait_recv()
-        for i in range(1, sp):
-            for left in range(2):
-                o = s + (2 * left - 1) * i
-
-                @pl.when((o >= 0) & (o < sp))
-                def _():
-                    for k in range(cuts):
-                        for j in range(1, grp):
-                            y_copy(l, j, o, (g + j) % grp, k).wait_recv()
+            for b in range(bands):
+                g_copy(l, b, sibling, p).wait_recv()
+        for j in range(1, grp):
+            all_of(wo.at[l, pl.ds(0, sp - 1), 0], y_recv.at[l, (g + j) % grp]).wait_recv()
 
         sq_sum[...] = jnp.zeros_like(sq_sum)
 
@@ -688,72 +701,70 @@
     for l in range(layers):
         layer_of(l)
 
+    def sent(block, sem):
+        all_of(block, sem).wait_send()
+
+    def sent_some(count, most, block, sem):
+        for n in range(1, most + 1):
+
+            @pl.when(count == n)
+            def _():
+                sent(block(n), sem)
+
     for l in range(layers):
-        for j in range(1, tp):
-            a_copy(l, (c + j) % tp, c).wait_send()
-            q_copy(l, (c + j) % tp, c).wait_send()
-            s_copy(l, (c + j) % tp, c).wait_send()
-        each(lambda j, left, d: b_copy(l, d, s).wait_send())
-
-        def sent(d):
-            c_copy(l, sibling, d, c_send.at[l, 0, d]).wait_send()
+        sent(pieces.at[l, pl.ds(0, tp - 1)], a_send.at[l])
+        sent(sq.at[l, pl.ds(0, tp - 1)], q_send.at[l])
+        sent(spread.at[l, pl.ds(0, sp - 1)], b_send.at[l])
+        for b in range(bands):
+            sent(stat.at[l, b, pl.ds(0, tp - 1)], s_send.at[l, b])
+            sent(acts.at[l, pl.ds(0, tp - 1), pl.ds(b * band, band)], g_send.at[l, b])
+
+        def exchanged(n):
+            for j in range(pairs):
+                sent(xs.at[l, 0, pl.ds(0, n)], c_send.at[l, j])
             for j in range(1, pairs):
-                p = (c + 2 * j) % tp
-                c_copy(l, p, d, c_send.at[l, j, d]).wait_send()
-                relay(l, p, d).wait_send()
-
-        sent(s)
-        each(lambda j, left, d: sent(d))
+                sent(xs.at[l, 0, pl.ds(0, n)], c_relay.at[l, (c + 2 * j) % tp])
+
         if lends(l):
+            for host in (False, True):
+
+                @pl.when(at_host == host)
+                def _():
+                    exchanged(sp + host)
 
             @pl.when(at_host)
             def _():
-                sent(sp)
-                for t in range(2 * lots):
-                    for j in range(1, grp):
-                        u_copy(l, j, t, g).wait_send()
+                for j in range(1, grp):
+                    sent(lot_of(l), u_send.at[l - 1, j])
 
             @pl.when(at_end)
             def _():
-                for t in range(2 * lots):
-                    v_copy(l, t).wait_send()
-
-
-        def partial_sent(j, left, d):
-            def one(slot, carry):
-                r_copy(l, left, d, slot).wait_send()
-                return carry
-
-            lax.fori_loop(0, 2 * sent_chunks(l, d), one, 0)
-
-        each(partial_sent)
+                sent(lot_of(l), v_send.at[l - 1])
+        else:
+            exchanged(sp)
+
+        for left in range(2):
+            for slot in range(2 * chunks):
+                skipped = at_end.astype(jnp.int32) * int(lends(l) and slot >= 2 * kept)
+                sent_some(
+                    beyond(left) - skipped,
+                    sp - 1,
+                    lambda n: going.at[l, left, pl.ds(0, n), slot],
+                    r_send.at[l, left, slot],
+                )
+            sent_some(
+                (behind(left) + 1) * (beyond(left) > 0).astype(jnp.int32),
+                sp - 1,
+                lambda n: wo.at[l, pl.ds(0, n), 0],
+                z_send.at[l, left],
+            )
+        for j in range(1, grp):
+            sent(wo.at[l, pl.ds(0, sp - 1), 0], y_send.at[l, j])
 
         @pl.when(s < sp - 1)
         def _():
             for i in range(chunks):
                 h_copy(l, s + 1, i).wait_send()
-
-        for i in range(sp):
-            for left in range(2):
-                o = s + (2 * left - 1) * i
-
-                @pl.when((o >= 0) & (o < sp))
-                def _():
-                    for k in range(cuts):
-
-                        @pl.when(beyond(left) > 0)
-                        def _():
-                            z_copy(l, left, o, k).wait_send()
-
-                        if i > 0:
-                            for j in range(1, grp):
-                                y_copy(l, j, o, g, k).wait_send()
-
-        g_copy(l, sibling, c, g_send.at[l, 0]).wait_send()
-        for j in range(1, pairs):
-            p = (c + 2 * j) % tp
-            g_copy(l, p, c, g_send.at[l, j]).wait_send()
-            g_copy(l, sibling, p, g_relay.at[l, p]).wait_send()
 
 
 def fused(tokens, rms_gain, w_value, w_gate, taps, ln_gain, ln_bias, w_out):
@@ -766,6 +777,7 @@
     pad = -(-(reach - 1) // 16) * 16
     share = w_out.shape[1] // grp
     cuts = CUTS
+    bands = 2 if rows % 32 == 0 and rows // 2 >= pad else 1
     vmem, dma = pltpu.VMEM, pltpu.SemaphoreType.DMA
     there = pl.BlockSpec(memory_space=pltpu.HBM)
     return pl.pallas_call(
@@ -791,23 +803,22 @@
             vmem((2, rows, step), F32),
             vmem((layers, tp, 8, padded), F32),
             vmem((rows, LANES), F32),
-            vmem((layers, tp, 8, padded), F32),
+            vmem((layers, bands, tp, 8, -(-rows // bands // LANES) * LANES), F32),
             vmem((layers, chans // step, pad, step), BF16),
             vmem((layers, chans // step, pad, step), BF16),
             vmem((pad + rows, chans), F32),
             vmem((rows, chans), F32),
             vmem((layers, tp, rows, chans), BF16),
             dma((5,)), dma((layers, 2)),
-            dma((layers, tp)), dma((layers, tp)), dma((layers, sp)),
-            dma((layers, tp, sp + 1)), dma((layers, tp, sp + 1)), dma((layers, tp, sp + 1)),
-            dma((layers, 2, sp, slots)), dma((layers, 2, sp, slots)),
-            dma((layers, tp)), dma((layers, tp)), dma((layers, tp)), dma((layers, tp)),
+            dma((layers,)), dma((layers, tp)), dma((layers,)),
+            dma((layers, tp // 2)), dma((layers, tp)), dma((layers, tp, sp + 1)),
+            dma((layers, 2, slots)), dma((layers, 2, sp, slots)),
+            dma((layers,)), dma((layers,)), dma((layers, bands)), dma((layers, bands)),
             dma((layers, chans // step)), dma((layers, chans // step)),
-            dma((layers, tp)), dma((layers, tp)), dma((layers, tp)),
-            dma((layers, grp)), dma((layers, 2, sp, cuts)), dma((layers, sp, cuts)),
-            dma((layers, grp, sp, cuts)), dma((layers, sp, grp, cuts)),
-            dma((layers, 2, LOTS)), dma((layers, 2, LOTS)),
-            dma((layers, grp, 2, LOTS)), dma((layers, 2, grp, LOTS)),
+            dma((layers, bands)), dma((layers, tp, bands)),
+            dma((layers, grp)), dma((layers, 2)), dma((layers, sp, cuts)),
+            dma((layers, grp)), dma((layers, grp)),
+            dma((layers,)), dma((layers, 2, LOTS)), dma((layers, grp)), dma((layers, grp)),
         ],
         compiler_params=pltpu.CompilerParams(
             collective_id=0, has_side_effects=True, vmem_limit_bytes=60 * 2**20

time: 152 us -> 144 us (0.947)
  Pallas kernels: 149 us -> 141 us
    pallas_call x1, Pallas kernels: 149 us -> 141 us  [fused(): pl.pallas_call(functools.partial(gated_conv, layers, sp, tp), out_shape=j...]
where the time goes in v4:
time: 144 us; the launch traced here: 143 us
  Pallas kernels  141 us (98%)
  local copies, waits for them, and re-layouts  1.82 us (1%)
    pallas_call x1, Pallas kernels, fused(): pl.pallas_call(functools.partial(gated_conv, layers, sp, tp), out_shape=j...  141 us

profile of v4, /device:TPU:24, one launch (start us, length us, event | category | flops | bytes accessed | tf_op | source)
XLA Modules:
  0.0 142.7 jit_solution(5088573137419343231)
XLA Ops:
  0.0 140.9 %shard_map.82 = bf16[224,1024]{1,0:T(8,128)(2,1)} custom-call(bf16[224,1024]{1,0:T(8,128)(2,1)} %h_hbm.1, f32[2,4096]{1,0:T(2,128)} %gain_hbm.1, bf16[2,1024,512]{2,1,0:T(8,128)(2,1)} %wv_hbm.1, bf16[2,1024,512]{2,1,0:T(8,128)(2,1)} %wg_hbm.1, f32[31,2,512]{2,1,0:T(2,128)} %bitcast.1, f32[2,512]{1,0:T(2,128)} %lng_hbm.1, f32[2,512]{1,0:T(2,128)} %lnb_hbm.1, ...), custom_call_target="tpu_custom_call" | custom-call | tf_op jit(solution)/shard_map/pallas_call | solution.py:783
  140.9 1.8 %copy.10 = bf16[224,1024]{1,0:T(8,128)(2,1)} copy(bf16[224,1024]{1,0:T(8,128)(2,1)} %shard_map.82) | data formatting | bytes 917504

commit v5 on v4

--- a/solution.py
+++ b/solution.py
@@ -17,7 +17,7 @@
     (2, 0): ("start", "start", "scattered", "turned"),
     (3, 0): ("start", "start", "scattered", "finished"),
     (0, 1): ("gathered", "gathered", "summed", "summed"),
-    (1, 1): ("gathered", "gathered", "summed", "summed"),
+    (1, 1): ("gathered", "gathered", "turned summed", "summed"),
     (2, 1): ("gathered summed", "gathered finished", "gathered finished", "counted"),
     (0, 2): ("summed", "summed", "counted", "counted"),
     (1, 2): ("counted", "counted", "closed", "closed"),
@@ -28,10 +28,12 @@
     (3, 0): ("tail", "tail", "tail", "tail"),
     (0, 1): ("gathered", "gathered", "gathered", "gathered"),
     (1, 1): ("before", "before", "gathered", "gathered"),
-    (2, 1): ("start", "before", "scattered", "finished"),
+    (2, 1): ("start", "before", "scattered", "scattered"),
     (0, 2): ("summed", "summed", "summed", "summed"),
-    (1, 2): ("summed", "summed", "counted", "counted"),
-    (0, 3): ("counted", "counted", "closed", "closed"),
+    (1, 2, 0): ("summed", "summed", "finished", "finished"),
+    (1, 2, 1): ("summed", "summed", "summed", "summed"),
+    (0, 3, 0): ("counted", "counted", "closed", "closed"),
+    (0, 3, 1): ("counted", "counted", "counted", "closed"),
 }
 
 
@@ -237,12 +239,12 @@
         for j in range(1, grp):
             y_copy(l, j, o, g, k).start()
 
-    def moment(l, ahead, i, k):
+    def moment(l, left, ahead, i, k):
         if l == 0:
             table = FIRST
         else:
             table = LATER
-        points = table.get((ahead, i), ("closed",) * 4)[4 * k // cuts]
+        points = table.get((ahead, i, left), table.get((ahead, i), ("closed",) * 4))[4 * k // cuts]
         return points.split() if " " in points else (points, points)
 
     def fill(l, point):
@@ -251,7 +253,7 @@
                 steps = []
                 for i in range(sp - ahead):
                     for k in range(cuts):
-                        taken, sent_on = moment(l, min(ahead, 3), i, k)
+                        taken, sent_on = moment(l, left, min(ahead, 3), i, k)
                         if i > 0 and taken == point:
                             steps.append((i, k, True))
                         if ahead > 0 and sent_on == point:
@@ -361,7 +363,7 @@
             going.at[l, left, d, slot],
             coming.at[l, left, d, slot],
             r_send.at[l, left, slot],
-            r_recv.at[l, left, d, slot],
+            r_recv.at[l, d + 1 - left, slot],
             sp=s + 1 - 2 * left,
         )
 
@@ -446,7 +448,7 @@
                 going.at[l, left, d, slot],
                 coming.at[l, left, d, slot],
                 r_send.at[l, left, slot],
-                r_recv.at[l, left, d, slot],
+                r_recv.at[l, d + 1 - left, slot],
                 sp=(s + 1) % sp,
             ).wait_recv()
 
@@ -812,7 +814,7 @@
             dma((5,)), dma((layers, 2)),
             dma((layers,)), dma((layers, tp)), dma((layers,)),
             dma((layers, tp // 2)), dma((layers, tp)), dma((layers, tp, sp + 1)),
-            dma((layers, 2, slots)), dma((layers, 2, sp, slots)),
+            dma((layers, 2, slots)), dma((layers, sp + 1, slots)),
             dma((layers,)), dma((layers,)), dma((layers, bands)), dma((layers, bands)),
             dma((layers, chans // step)), dma((layers, chans // step)),
             dma((layers, bands)), dma((layers, tp, bands)),

time: 144 us -> 143 us (level)
  no operation moved by 1% of the time
where the time goes in v5:
time: 143 us; the launch traced here: 142 us
  Pallas kernels  141 us (99%)
  local copies, waits for them, and re-layouts  1.82 us (1%)
    pallas_call x1, Pallas kernels, fused(): pl.pallas_call(functools.partial(gated_conv, layers, sp, tp), out_shape=j...  141 us

profile of v5, /device:TPU:24, one launch (start us, length us, event | category | flops | bytes accessed | tf_op | source)
XLA Modules:
  0.0 142.5 jit_solution(4747572019938146610)
XLA Ops:
  0.0 140.7 %shard_map.82 = bf16[224,1024]{1,0:T(8,128)(2,1)} custom-call(bf16[224,1024]{1,0:T(8,128)(2,1)} %h_hbm.1, f32[2,4096]{1,0:T(2,128)} %gain_hbm.1, bf16[2,1024,512]{2,1,0:T(8,128)(2,1)} %wv_hbm.1, bf16[2,1024,512]{2,1,0:T(8,128)(2,1)} %wg_hbm.1, f32[31,2,512]{2,1,0:T(2,128)} %bitcast.1, f32[2,512]{1,0:T(2,128)} %lng_hbm.1, f32[2,512]{1,0:T(2,128)} %lnb_hbm.1, ...), custom_call_target="tpu_custom_call" | custom-call | tf_op jit(solution)/shard_map/pallas_call | solution.py:785
  140.7 1.8 %copy.10 = bf16[224,1024]{1,0:T(8,128)(2,1)} copy(bf16[224,1024]{1,0:T(8,128)(2,1)} %shard_map.82) | data formatting | bytes 917504

commit v6 on v5

--- a/solution.py
+++ b/solution.py
@@ -32,7 +32,7 @@
     (0, 2): ("summed", "summed", "summed", "summed"),
     (1, 2, 0): ("summed", "summed", "finished", "finished"),
     (1, 2, 1): ("summed", "summed", "summed", "summed"),
-    (0, 3, 0): ("counted", "counted", "closed", "closed"),
+    (0, 3, 0): ("counted", "counted", "counted", "closed"),
     (0, 3, 1): ("counted", "counted", "counted", "closed"),
 }
 
@@ -213,7 +213,7 @@
             wo.at[l, o, g, rows_k],
             wo.at[l, o, g, rows_k],
             z_send.at[l, left],
-            z_recv.at[l, o, k],
+            z_recv.at[l, o - (o > s + 1 - 2 * left).astype(jnp.int32), k],
             sp=s + 1 - 2 * left,
         )
 
@@ -233,7 +233,7 @@
             wo.at[l, o, g, rows_k],
             wo.at[l, o, g, rows_k],
             z_send.at[l, 0],
-            z_recv.at[l, o, k],
+            z_recv.at[l, o - (o > s).astype(jnp.int32), k],
             sp=(s + 1) % sp,
         ).wait_recv()
         for j in range(1, grp):
@@ -818,7 +818,7 @@
             dma((layers,)), dma((layers,)), dma((layers, bands)), dma((layers, bands)),
             dma((layers, chans // step)), dma((layers, chans // step)),
             dma((layers, bands)), dma((layers, tp, bands)),
-            dma((layers, grp)), dma((layers, 2)), dma((layers, sp, cuts)),
+            dma((layers, grp)), dma((layers, 2)), dma((layers, sp - 1, cuts)),
             dma((layers, grp)), dma((layers, grp)),
             dma((layers,)), dma((layers, 2, LOTS)), dma((layers, grp)), dma((layers, grp)),
         ],

time: 143 us -> 142 us (level)
  no operation moved by 1% of the time
where the time goes in v6:
time: 142 us
  Pallas kernels  140 us (99%)
  local copies, waits for them, and re-layouts  1.82 us (1%)
    pallas_call x1, Pallas kernels, fused(): pl.pallas_call(functools.partial(gated_conv, layers, sp, tp), out_shape=j...  140 us

profile of v6, /device:TPU:24, one launch (start us, length us, event | category | flops | bytes accessed | tf_op | source)
XLA Modules:
  0.0 142.3 jit_solution(11561912042603108650)
XLA Ops:
  0.0 140.5 %shard_map.82 = bf16[224,1024]{1,0:T(8,128)(2,1)} custom-call(bf16[224,1024]{1,0:T(8,128)(2,1)} %h_hbm.1, f32[2,4096]{1,0:T(2,128)} %gain_hbm.1, bf16[2,1024,512]{2,1,0:T(8,128)(2,1)} %wv_hbm.1, bf16[2,1024,512]{2,1,0:T(8,128)(2,1)} %wg_hbm.1, f32[31,2,512]{2,1,0:T(2,128)} %bitcast.1, f32[2,512]{1,0:T(2,128)} %lng_hbm.1, f32[2,512]{1,0:T(2,128)} %lnb_hbm.1, ...), custom_call_target="tpu_custom_call" | custom-call | tf_op jit(solution)/shard_map/pallas_call | solution.py:785
  140.5 1.8 %copy.10 = bf16[224,1024]{1,0:T(8,128)(2,1)} copy(bf16[224,1024]{1,0:T(8,128)(2,1)} %shard_map.82) | data formatting | bytes 917504
